TPU v7x, 512 devices: a whole 4x4x16 slice. The times are simulated.
512 devices in a mesh: ep: 32 (over z, core), tp: 16 (over y, x).
Axes of the slice: x: 4, y: 4, z: 16, core: 2. Of those that a mesh axis runs over, the one named last changes fastest.
Arguments:
- compressed_query: bfloat16 [4096, 1536], P('ep'), may hold values from -6 to 6
- compressed_key_value: bfloat16 [4096, 512], P('ep'), may hold values from -6 to 6
- rotary_key: bfloat16 [4096, 32], P('ep'), may hold values from -600 to 600
- query_norm_scale: float32 [1536], replicated, may hold values from 0.1 to 1.9
- context_norm_scale: float32 [512], replicated, may hold values from 0.1 to 1.9
- query_plain_weight: bfloat16 [1536, 1024], P(None, 'tp'), may hold values from -0.375 to 0.375
- query_rotary_weight: bfloat16 [1536, 512], P(None, 'tp'), may hold values from -0.375 to 0.375
- key_up_weight: bfloat16 [512, 1024], P(None, 'tp'), may hold values from -0.25 to 0.25
- value_up_weight: bfloat16 [512, 1024], P(None, 'tp'), may hold values from -0.25 to 0.25
- output_weight: bfloat16 [1024, 2048], P(None, 'tp'), may hold values from -0.75 to 0.75
- mixture_input: bfloat16 [4096, 2048], P('ep'), may hold values from -6 to 6
- mixture_gain: float32 [2048], replicated, may hold values from 0.1 to 1.9
- routes: int32 [4096, 2], P('ep'), may hold values from 0 to 31, all different within a row; in each aligned block of 128 rows (0 to 127, 128 to 255, ...) at most 12 rows name the same one
- route_weight: float32 [4096, 2], P('ep'), may hold values from 0.2 to 2
- expert_gate: bfloat16 [32, 2048, 4096], P('ep', None, 'tp'), may hold values from -0.125 to 0.125
- expert_up: bfloat16 [32, 2048, 4096], P('ep', None, 'tp'), may hold values from -0.125 to 0.125
- expert_down: bfloat16 [32, 4096, 2048], P('ep', None, 'tp'), may hold values from -0.09375 to 0.09375
- shared_gate: bfloat16 [2048, 512], P(None, 'tp'), may hold values from -0.125 to 0.125
- shared_up: bfloat16 [2048, 512], P(None, 'tp'), may hold values from -0.125 to 0.125
- shared_down: bfloat16 [512, 2048], P(None, 'tp'), may hold values from -0.25 to 0.25
Outputs:
- attended: bfloat16 [4096, 2048], P('ep', 'tp')
- combined: bfloat16 [4096, 2048], P('ep', 'tp')
Inputs may be any that keep to these rules, and one draw needn't show every extreme that they name: `routes`: in the rows of each index of ep, no expert is named more than 12 times, a bound that some block reaches there.
All inputs are finite; a program needn't handle non-finite values.
Results may differ from a plain program's by a relative error of at most 0.012.
The roundings to bfloat16 on the way count: a program that leaves them out, or rounds other values in their place, can miss the bound.
Values may be sent and summed in bfloat16 or wider, within the bound.
No kernel may reach another device: no remote copies, remote signals or barrier semaphores. Data moves between devices by JAX's collectives and lax.ppermute only.
A program may use at most 64 MiB of HBM per device.

v0:
```python
import math

import jax
import jax.numpy as jnp
from jax import lax
from jax.sharding import Mesh
from jax.sharding import PartitionSpec as P

PLAIN_HEAD_SIZE = 64
ROTARY_SIZE = 32
VALUE_HEAD_SIZE = 64
TOPK = 2
EP = ("ep_0", "ep_1")


def sent_together(arrays, axis, dim, along):
    widths = [a.shape[along] for a in arrays]
    both = jnp.concatenate(arrays, axis=along)
    filled = lax.all_gather(both, axis, axis=dim, tiled=True)
    return tuple(jnp.split(filled, [sum(widths[:k]) for k in range(1, len(widths))], axis=along))


def from_everyone(array, axis):
    copies = jnp.broadcast_to(array, (lax.axis_size(axis), *array.shape))
    return lax.all_to_all(copies, axis, split_axis=0, concat_axis=0, tiled=True)


def joined_along(parts, dim):
    parts = jnp.moveaxis(parts, 0, dim)
    shape = parts.shape
    return parts.reshape(*shape[:dim], shape[dim] * shape[dim + 1], *shape[dim + 2 :])


def gather_directly(array, axis, dim):
    parts = from_everyone(array, axis)
    return joined_along(parts, dim)


def cut_along(array, dim, devices):
    shape = array.shape
    parts = array.reshape(*shape[:dim], devices, shape[dim] // devices, *shape[dim + 1 :])
    return jnp.moveaxis(parts, dim, 0)


def moved_by_axis(parts, axes, sequence):
    inside = parts.shape[1:]
    filled = parts.reshape(*(lax.axis_size(a) for a in axes), *inside)
    for k in sequence:
        filled = lax.all_to_all(filled, axes[k], k, k, tiled=True)
    return filled.reshape(-1, *inside)


def exchange_by_chip(array, groups, sequence, split_dim, concat_dim):
    devices = lax.axis_size(groups[0]) * lax.axis_size(groups[1])
    parts = cut_along(array, split_dim, devices)
    return joined_along(moved_by_axis(parts, groups, sequence), concat_dim)


def normed_rows(values, scaling):
    floats = values.astype(jnp.float32)
    return floats * lax.rsqrt(jnp.mean(floats * floats, axis=-1, keepdims=True) + 1e-06) * scaling


def rotary_tables(positions):
    inverse = 1.0 / 10000.0 ** (jnp.arange(0, ROTARY_SIZE, 2, dtype=jnp.float32) / ROTARY_SIZE)
    angles = positions.astype(jnp.float32)[:, None] * inverse[None, :]
    return (jnp.cos(angles), jnp.sin(angles))


def rotate(vectors, cosine, sine_part):
    half_width = vectors.shape[-1] // 2
    front_half = vectors[..., :half_width]
    back_half = vectors[..., half_width:]
    return jnp.concatenate(
        [front_half * cosine - back_half * sine_part, front_half * sine_part + back_half * cosine],
        axis=-1,
    )


def fold_blocks(carry_state, members, handle):
    length = members[0].shape[0]
    block_rows = math.gcd(length, 2048)

    def advance(block_index, carried):
        sliced = tuple(
            (
                lax.dynamic_slice_in_dim(member, block_index * block_rows, block_rows, 0)
                for member in members
            )
        )
        return handle(carried, sliced, block_index * block_rows)

    return lax.fori_loop(0, length // block_rows, advance, carry_state)


def per_device(
    compressed_query,
    compressed_key_value,
    rotary_key,
    query_norm_scale,
    context_norm_scale,
    query_plain_weight,
    query_rotary_weight,
    key_up_weight,
    value_up_weight,
    output_weight,
    mixture_input,
    mixture_gain,
    routes,
    route_weight,
    expert_gate,
    expert_up,
    expert_down,
    shared_gate,
    shared_up,
    shared_down,
):
    tokens = compressed_query.shape[0]
    heads_here = query_plain_weight.shape[1] // PLAIN_HEAD_SIZE
    offset = lax.axis_index(EP) * tokens
    cosine, sine_part = rotary_tables(offset + jnp.arange(tokens, dtype=jnp.int32))
    compressed = normed_rows(compressed_query, query_norm_scale).astype(jnp.bfloat16)
    query_nope = jnp.dot(compressed, query_plain_weight, preferred_element_type=jnp.float32)
    query_nope = query_nope.astype(jnp.bfloat16).reshape(tokens, heads_here, PLAIN_HEAD_SIZE)
    query_turn = jnp.dot(compressed, query_rotary_weight, preferred_element_type=jnp.float32)
    query_turn = query_turn.reshape(tokens, heads_here, ROTARY_SIZE)
    query_rot = rotate(query_turn, cosine[:, None, :], sine_part[:, None, :])
    context = normed_rows(compressed_key_value, context_norm_scale).astype(jnp.bfloat16)
    scale = (PLAIN_HEAD_SIZE + ROTARY_SIZE) ** (-0.5)
    start_state = (
        jnp.full((heads_here, tokens), -1e30, jnp.float32),
        jnp.zeros((heads_here, tokens), jnp.float32),
        jnp.zeros((heads_here, tokens, VALUE_HEAD_SIZE), jnp.float32),
    )

    def attend(carry_state, sliced, first_row):
        key_rows, value_rows, raw_turn = sliced
        count = raw_turn.shape[0]
        key_cos, key_sin = rotary_tables(first_row + jnp.arange(count, dtype=jnp.int32))
        turned = rotate(raw_turn.astype(jnp.float32), key_cos, key_sin)
        running_max, running_total, running_sum = carry_state
        key_heads = key_rows.reshape(count, heads_here, PLAIN_HEAD_SIZE)
        value_heads = value_rows.reshape(count, heads_here, VALUE_HEAD_SIZE)
        scores = (
            jnp.einsum("qhe,khe->hqk", query_nope, key_heads, preferred_element_type=jnp.float32)
            + jnp.einsum("qhr,kr->hqk", query_rot, turned, precision=lax.Precision.HIGHEST)
        ) * scale
        new_max = jnp.maximum(running_max, jnp.max(scores, axis=-1))
        factor = jnp.exp(running_max - new_max)
        weights = jnp.exp(scores - new_max[..., None])
        running_total = running_total * factor + jnp.sum(weights, axis=-1)
        running_sum = running_sum * factor[..., None] + jnp.einsum(
            "hqk,khe->hqe",
            weights.astype(jnp.bfloat16),
            value_heads,
            preferred_element_type=jnp.float32,
        )
        return (new_max, running_total, running_sum)

    key_local = jnp.dot(context, key_up_weight, preferred_element_type=jnp.float32).astype(
        jnp.bfloat16
    )
    value_local = jnp.dot(context, value_up_weight, preferred_element_type=jnp.float32).astype(
        jnp.bfloat16
    )
    final_state = fold_blocks(
        start_state, sent_together((key_local, value_local, rotary_key), EP, 0, 1), attend
    )
    heads_out = final_state[2] / final_state[1][..., None]
    heads_out = (
        heads_out.transpose(1, 0, 2)
        .reshape(tokens, heads_here * VALUE_HEAD_SIZE)
        .astype(jnp.bfloat16)
    )
    all_heads = gather_directly(heads_out, "tp", 1)
    attended = jnp.dot(all_heads, output_weight, preferred_element_type=jnp.float32).astype(
        jnp.bfloat16
    )
    floats = mixture_input.astype(jnp.float32)
    centred = floats - jnp.mean(floats, axis=-1, keepdims=True)
    normed = (
        centred
        * lax.rsqrt(jnp.mean(centred * centred, axis=-1, keepdims=True) + 1e-05)
        * mixture_gain
    ).astype(jnp.bfloat16)
    experts = lax.axis_size(EP)
    rows_here = mixture_input.shape[0]
    model_width = normed.shape[1]
    capacity = rows_here * TOPK * 3 // (2 * experts)
    flat_routes = routes.reshape(-1)
    one_hot = (flat_routes[:, None] == jnp.arange(experts, dtype=jnp.int32)[None, :]).astype(
        jnp.int32
    )
    ranks = jnp.sum(one_hot * (jnp.cumsum(one_hot, axis=0) - 1), axis=1)
    slots = flat_routes * capacity + ranks
    owners = jnp.full((experts * capacity,), rows_here, jnp.int32)
    owners = owners.at[slots].set(jnp.arange(rows_here * TOPK, dtype=jnp.int32) // TOPK)
    padded = jnp.concatenate([normed, jnp.zeros((1, model_width), jnp.bfloat16)], axis=0)
    outgoing = padded[owners].reshape(experts, capacity, model_width)
    width_here = model_width // lax.axis_size("tp")
    own_columns = lax.dynamic_slice_in_dim(
        outgoing, lax.axis_index("tp") * width_here, width_here, 2
    )
    moved = exchange_by_chip(own_columns, ("ep_0", "ep_1"), (1, 0), 0, 0)
    arrived = gather_directly(moved, "tp", 2).reshape(experts * capacity, model_width)
    hidden = (
        jax.nn.silu(jnp.dot(arrived, expert_gate[0], preferred_element_type=jnp.float32))
        * jnp.dot(arrived, expert_up[0], preferred_element_type=jnp.float32)
    ).astype(jnp.bfloat16)
    shared_hidden = (
        jax.nn.silu(jnp.dot(normed, shared_gate, preferred_element_type=jnp.float32))
        * jnp.dot(normed, shared_up, preferred_element_type=jnp.float32)
    ).astype(jnp.bfloat16)
    all_hidden, all_shared = (
        lax.all_gather(hidden, "tp", axis=1, tiled=True),
        lax.all_gather(shared_hidden, "tp", axis=1, tiled=True),
    )
    expert_rows = jnp.dot(all_hidden, expert_down[0], preferred_element_type=jnp.float32).astype(
        jnp.bfloat16
    )
    features = expert_rows.shape[1]
    returned = lax.all_to_all(
        expert_rows.reshape(experts, capacity, features),
        EP,
        split_axis=0,
        concat_axis=0,
        tiled=True,
    )
    picked = returned.reshape(experts * capacity, features)[slots]
    picked = picked.astype(jnp.float32).reshape(rows_here, TOPK, features)
    routed = jnp.sum(picked * route_weight[:, :, None], axis=1)
    combined = (
        jnp.dot(all_shared, shared_down, preferred_element_type=jnp.float32) + routed
    ).astype(jnp.bfloat16)
    return (attended, combined)


def solution(mesh):
    split = Mesh(mesh.devices.reshape(16, 2, mesh.shape["tp"]), ("ep_0", "ep_1", "tp"))
    placed = (
        P(EP, None),
        P(EP, None),
        P(EP, None),
        P(),
        P(),
        P(None, "tp"),
        P(None, "tp"),
        P(None, "tp"),
        P(None, "tp"),
        P(None, "tp"),
        P(EP, None),
        P(),
        P(EP, None),
        P(EP, None),
        P(EP, None, "tp"),
        P(EP, None, "tp"),
        P(EP, None, "tp"),
        P(None, "tp"),
        P(None, "tp"),
        P(None, "tp"),
    )
    return jax.shard_map(
        per_device,
        mesh=split,
        in_specs=placed,
        out_specs=(P(EP, "tp"), P(EP, "tp")),
        check_vma=False,
    )
```

profile of v0, /device:TPU:32, one launch (start us, length us, event | category | flops | bytes accessed | tf_op | source)
XLA Modules:
  0.0 203.8 jit_solution(6303473460601406312)
XLA Ops:
  7.2 1.1 fusion.52
  8.4 1.2 convolution_convert_fusion.2
  9.5 1.2 convolution_convert_fusion.3
  10.7 1.3 pad_maximum_fusion
  12.1 0.7 broadcast_multiply_fusion
  12.8 0.8 copy.66
  13.8 1.2 convert_reduce_fusion
  16.6 1.4 scatter_custom_fusion
  18.4 3.1 %gather_fusion = bf16[384,2048]{1,0:T(8,128)(2,1)} fusion(bf16[129,2048]{1,0:T(8,128)(2,1)S(1)} %concatenate.21, s32[1024]{0:T(1024)S(1)} %pad_clamp_fusion.1), kind=kCustom, calls=%fused_computation | custom fusion | bytes 3147264 | tf_op jit(solution)/shard_map/gather | solution.py:199
  21.5 3.6 %reshape.297 = bf16[32,12,2048]{2,1,0:T(8,128)(2,1)} reshape(bf16[384,2048]{1,0:T(8,128)(2,1)} %gather_fusion) | data formatting | bytes 3145728 | tf_op jit(solution)/shard_map/reshape | solution.py:199
  25.1 0.9 constant_dynamic-slice_fusion
  26.1 3.8 %all_to_all.25 = bf16[16,2,1,12,128]{4,0,3,2,1:T(8,128)(2,1)S(1)} all-to-all(bf16[16,2,1,12,128]{4,0,3,2,1:T(8,128)(2,1)S(1)} %copy.70), channel_id=1, replica_groups=mesh['ep_0'=16,'ep_1'=2,'tp'=16] {'ep_1'}, dimensions={1} | all-to-all | bytes 196608 | tf_op jit(solution)/shard_map/all_to_all | solution.py:49
  30.0 27.9 %all_to_all.26 = bf16[16,2,1,12,128]{4,1,3,2,0:T(2,128)(2,1)S(1)} all-to-all(bf16[16,2,1,12,128]{4,1,3,2,0:T(2,128)(2,1)S(1)} %copy.71), channel_id=1, replica_groups=mesh['ep_0'=16,'ep_1'=2,'tp'=16] {'ep_0'}, dimensions={0} | all-to-all | bytes 196608 | tf_op jit(solution)/shard_map/all_to_all | solution.py:49
  57.9 1.5 broadcast_in_dim.56
  59.4 7.2 %all-to-all-start.3 = ((bf16[16,32,12,128]{3,1,2,0:T(8,128)(2,1)}), bf16[16,32,12,128]{3,1,2,0:T(8,128)(2,1)}, u32[]{:S(2)}, u32[]{:S(2)}) async-start(bf16[16,32,12,128]{3,1,2,0:T(8,128)(2,1)} %broadcast_in_dim.56), calls=%async_computation.3 | async-start | bytes 3145728 | tf_op jit(solution)/shard_map/all_to_all | solution.py:25
  67.6 21.7 %all-to-all-done.3 = bf16[16,32,12,128]{3,1,2,0:T(8,128)(2,1)} async-done(((bf16[16,32,12,128]{3,1,2,0:T(8,128)(2,1)}), bf16[16,32,12,128]{3,1,2,0:T(8,128)(2,1)}, u32[]{:S(2)}, u32[]{:S(2)}) %all-to-all-start.3) | async-done | bytes 1572896 | tf_op jit(solution)/shard_map/all_to_all | solution.py:25
  89.3 2.4 %copy.73 = bf16[32,12,16,128]{3,2,1,0:T(8,128)(2,1)S(1)} copy(bf16[32,12,16,128]{3,0,1,2:T(8,128)(2,1)} %bitcast.11) | data formatting | bytes 3145728 | tf_op jit(solution)/shard_map/transpose | solution.py:29
  93.0 1.3 fusion.37
  94.5 0.7 copy.74
  95.8 1.3 fusion.73
  97.2 7.2 %while.20 = (s32[]{:T(128)}, f32[1,128]{1,0:T(1,128)S(1)}, f32[1,128]{1,0:T(1,128)S(1)}, f32[1,128,64]{1,2,0:T(8,128)S(1)}, bf16[4096,64]{0,1:T(8,128)(2,1)S(1)}...) while((s32[]{:T(128)}, f32[1,128]{1,0:T(1,128)S(1)}, ...), condition=%wide.region_5.0_spmd.clone, body=%wide.region_2.0_spmd.clone.sunk | while | flops 169997088 | bytes 7070031 | solution.py:93
  97.8 1.8 convolution_bitcast_fusion.5
  101.4 1.8 convolution_bitcast_fusion.5
  104.4 0.8 broadcast_in_dim.29
  105.2 3.7 %all-to-all-start = ((bf16[16,128,64]{1,2,0:T(8,128)(2,1)}), bf16[16,128,64]{1,2,0:T(8,128)(2,1)S(1)}, u32[]{:S(2)}, u32[]{:S(2)}) async-start(bf16[16,128,64]{1,2,0:T(8,128)(2,1)} %broadcast_in_dim.29), calls=%async_computation | async-start | bytes 524288 | tf_op jit(solution)/shard_map/all_to_all | solution.py:25
  108.9 45.7 %all-gather.5.cloned.1.call-done = bf16[384,4096]{1,0:T(8,128)(2,1)} async-done(((bf16[384,256]{1,0:T(8,128)(2,1)}), bf16[384,4096]{1,0:T(8,128)(2,1)}) %all-gather.5.cloned.1.call-update) | async-done | bytes 3145744 | tf_op jit(solution)/shard_map/all_gather | solution.py:215
  154.6 2.9 %convolution_convert_fusion = bf16[384,128]{1,0:T(8,128)(2,1)S(1)} fusion(bf16[384,4096]{1,0:T(8,128)(2,1)} %all-gather.5.cloned.1.call-done, bf16[1,4096,128]{2,1,0:T(8,128)(2,1)S(1)} %copy-done.2), kind=kOutput, calls=%fused_computation.54 | convolution fusion | flops 402702336 | bytes 4292608 | tf_op jit(solution)/shard_map/dot_general | solution.py:218
  158.2 12.8 %all-to-all-start.4 = ((bf16[32,12,128]{2,1,0:T(8,128)(2,1)}), bf16[32,12,128]{2,1,0:T(8,128)(2,1)S(1)}, u32[]{:S(2)}, u32[]{:S(2)}) async-start(bf16[32,12,128]{2,1,0:T(8,128)(2,1)} %reshape.298), calls=%async_computation.4 | async-start | bytes 262144 | tf_op jit(solution)/shard_map/all_to_all | solution.py:222
  171.0 23.1 %all_gather.10 = bf16[128,512]{0,1:T(8,128)(2,1)S(1)} all-gather(bf16[128,32]{0,1:T(8,128)(2,1)S(1)} %fusion.42), channel_id=1, replica_groups=mesh['ep_0'=16,'ep_1'=2,'tp'=16] {'tp'}, dimensions={1}, use_global_device_ids=true | all-gather | bytes 139264 | tf_op jit(solution)/shard_map/all_gather | solution.py:216
  194.1 0.9 convolution_convert_fusion.1
  195.0 0.9 gather_fusion.1
  196.1 0.8 fusion.40
  (102 shorter events, 9.8 us)
Async XLA Ops:
  7.2 84.6 %copy-start = (bf16[1,2048,256]{2,1,0:T(8,128)(2,1)S(1)}, bf16[1,2048,256]{2,1,0:T(8,128)(2,1)}, u32[]{:S(2)}) copy-start(bf16[1,2048,256]{2,1,0:T(8,128)(2,1)} %param.36) | copy-start | bytes 3145732
  7.2 7.9 %copy-start.1 = (bf16[128,2048]{1,0:T(8,128)(2,1)S(1)}, bf16[128,2048]{1,0:T(8,128)(2,1)}, u32[]{:S(2)}) copy-start(bf16[128,2048]{1,0:T(8,128)(2,1)} %param.32) | copy-start | bytes 1572868
  7.2 10.8 %copy-start.9 = (f32[2048]{0:T(1024)S(1)}, f32[2048]{0:T(1024)}, u32[]{:S(2)}) copy-start(f32[2048]{0:T(1024)} %param.33) | copy-start | bytes 24580
  7.2 88.6 %all-gather.3.cloned.1.call-start = ((), (), s32[]{:S(2)}) async-start(), calls=%async_computation.5 | async-start | bytes 1351680 | tf_op jit(solution)/shard_map/all_gather | solution.py:19
  59.4 7.3 %copy-start.3 = (bf16[128,1536]{1,0:T(8,128)(2,1)S(1)}, bf16[128,1536]{1,0:T(8,128)(2,1)}, u32[]{:S(2)}) copy-start(bf16[128,1536]{1,0:T(8,128)(2,1)} %param.22) | copy-start | bytes 1179652
  59.4 7.5 %copy-start.13 = (bf16[1536,32]{0,1:T(8,128)(2,1)S(1)}, bf16[1536,32]{0,1:T(8,128)(2,1)}, u32[]{:S(2)}) copy-start(bf16[1536,32]{0,1:T(8,128)(2,1)} %param.28) | copy-start | bytes 294916
  59.4 7.5 %copy-start.14 = (f32[1536]{0:T(1024)S(1)}, f32[1536]{0:T(1024)}, u32[]{:S(2)}) copy-start(f32[1536]{0:T(1024)} %param.25) | copy-start | bytes 18436
  59.4 8.0 %copy-start.6 = (bf16[2048,32]{0,1:T(8,128)(2,1)S(1)}, bf16[2048,32]{0,1:T(8,128)(2,1)}, u32[]{:S(2)}) copy-start(bf16[2048,32]{0,1:T(8,128)(2,1)} %param.39) | copy-start | bytes 393220
  59.4 29.9 %all-to-all-start.3 = ((bf16[16,32,12,128]{3,1,2,0:T(8,128)(2,1)}), bf16[16,32,12,128]{3,1,2,0:T(8,128)(2,1)}, u32[]{:S(2)}, u32[]{:S(2)}) async-start(bf16[16,32,12,128]{3,1,2,0:T(8,128)(2,1)} %broadcast_in_dim.56), calls=%async_computation.3 | async-start | bytes 3145728 | tf_op jit(solution)/shard_map/all_to_all | solution.py:25
  66.6 88.0 %all-gather.5.cloned.1.call-start = ((), (), s32[]{:S(2)}) async-start(), calls=%async_computation.6 | async-start | bytes 3342336 | tf_op jit(solution)/shard_map/all_gather | solution.py:215
  91.8 1.2 copy-start.11
  93.0 1.4 copy-start.10
  93.0 2.2 %copy-start.12 = (bf16[1536,64]{0,1:T(8,128)(2,1)S(1)}, bf16[1536,64]{0,1:T(8,128)(2,1)}, u32[]{:S(2)}) copy-start(bf16[1536,64]{0,1:T(8,128)(2,1)} %param.27) | copy-start | bytes 589828
  93.0 2.5 %copy-start.7 = (bf16[2048,32]{0,1:T(8,128)(2,1)S(1)}, bf16[2048,32]{0,1:T(8,128)(2,1)}, u32[]{:S(2)}) copy-start(bf16[2048,32]{0,1:T(8,128)(2,1)} %param.40) | copy-start | bytes 393220
  95.8 1.3 slice-start
  97.2 57.5 %copy-start.2 = (bf16[1,4096,128]{2,1,0:T(8,128)(2,1)S(1)}, bf16[1,4096,128]{2,1,0:T(8,128)(2,1)}, u32[]{:S(2)}) copy-start(bf16[1,4096,128]{2,1,0:T(8,128)(2,1)} %param.38) | copy-start | bytes 3145732
  105.2 53.0 %all-to-all-start = ((bf16[16,128,64]{1,2,0:T(8,128)(2,1)}), bf16[16,128,64]{1,2,0:T(8,128)(2,1)S(1)}, u32[]{:S(2)}, u32[]{:S(2)}) async-start(bf16[16,128,64]{1,2,0:T(8,128)(2,1)} %broadcast_in_dim.29), calls=%async_computation | async-start | bytes 524288 | tf_op jit(solution)/shard_map/all_to_all | solution.py:25
  108.9 85.2 %copy-start.5 = (bf16[1024,128]{1,0:T(8,128)(2,1)S(1)}, bf16[1024,128]{1,0:T(8,128)(2,1)}, u32[]{:S(2)}) copy-start(bf16[1024,128]{1,0:T(8,128)(2,1)} %param.31) | copy-start | bytes 786436
  157.5 38.4 %copy-start.4 = (f32[128,2]{1,0:T(8,128)S(1)}, f32[128,2]{1,0:T(8,128)}, u32[]{:S(2)}) copy-start(f32[128,2]{1,0:T(8,128)} %copy.74) | copy-start | bytes 3076
  157.5 38.6 %copy-start.8 = (bf16[512,128]{1,0:T(8,128)(2,1)S(1)}, bf16[512,128]{1,0:T(8,128)(2,1)}, u32[]{:S(2)}) copy-start(bf16[512,128]{1,0:T(8,128)(2,1)} %param.41) | copy-start | bytes 393220
  158.2 36.8 %all-to-all-start.4 = ((bf16[32,12,128]{2,1,0:T(8,128)(2,1)}), bf16[32,12,128]{2,1,0:T(8,128)(2,1)S(1)}, u32[]{:S(2)}, u32[]{:S(2)}) async-start(bf16[32,12,128]{2,1,0:T(8,128)(2,1)} %reshape.298), calls=%async_computation.4 | async-start | bytes 262144 | tf_op jit(solution)/shard_map/all_to_all | solution.py:222
Sparse Core Ops, SparseCore 0:
  12.2 76.0 all-gather.2
  94.4 60.1 all-gather.4
where the time goes:
time: 205 us; the launch traced here: 204 us
  waiting for transfers between devices  67.5 us (33%)
  blocking collectives  54.7 us (27%)
  starting transfers between devices  23.8 us (12%)
  local copies, waits for them, and re-layouts  19.8 us (10%)
  matrix products  15.2 us (7%)
  between operations  14.5 us (7%)
  other arithmetic  8.19 us (4%)
    all_gather x1, waiting for transfers between devices, per_device(): lax.all_gather(hidden, 'tp', axis=1, tiled=True)  45.7 us
    all_to_all x2, blocking collectives, moved_by_axis(): filled = lax.all_to_all(filled, axes[k], k, k, tiled=True)  31.7 us
    all_gather x1, blocking collectives, per_device(): lax.all_gather(shared_hidden, 'tp', axis=1, tiled=True)  23.1 us
    all_to_all x2, waiting for transfers between devices, from_everyone(): return lax.all_to_all(copies, axis, split_axis=0, concat_axis=0, tiled=True)  21.7 us
    all_to_all x1, starting transfers between devices, per_device(): lax.all_to_all(expert_rows.reshape(experts, capacity, features), EP, spli...  12.8 us
    all_to_all x2, starting transfers between devices, from_everyone(): return lax.all_to_all(copies, axis, split_axis=0, concat_axis=0, tiled=True)  10.9 us
  transfers between devices with their start and end apart: 5, of which 2 were waited for; matrix products, arithmetic and copies ran while one was open for 18% of the time, Pallas kernels for 0%

commit v1 on v0

v1 whole, which is shorter than its diff:
```python
import functools

import jax
import jax.numpy as jnp
import numpy as np
from jax import lax
from jax.experimental import pallas as pl
from jax.experimental.pallas import tpu as pltpu
from jax.sharding import Mesh
from jax.sharding import PartitionSpec as P

PLAIN = 64
ROTARY = 32
VALUE = 64
EP = ("z", "core")
TP = ("y", "x")
PLANE = ("core", "y", "x")
F32 = jnp.float32
BF16 = jnp.bfloat16
VMEM = pl.BlockSpec(memory_space=pltpu.VMEM)
SMEM = pl.BlockSpec(memory_space=pltpu.SMEM)


def dot(a, b, ca=1, cb=0):
    return lax.dot_general(a, b, (((ca,), (cb,)), ((), ())), preferred_element_type=F32)


def call(body, outs, args, smem=0, flops=10**9, bytes_accessed=10**6):
    return pl.pallas_call(
        body,
        out_shape=outs,
        in_specs=[SMEM] * smem + [VMEM] * (len(args) - smem),
        out_specs=jax.tree.map(lambda _: VMEM, outs),
        cost_estimate=pl.CostEstimate(
            flops=flops, bytes_accessed=bytes_accessed, transcendentals=0
        ),
    )(*args)


def shape(dims, dtype=BF16):
    return jax.ShapeDtypeStruct(dims, dtype)


def split3(x):
    high = x.astype(BF16)
    rest = x - high.astype(F32)
    middle = rest.astype(BF16)
    low = (rest - middle.astype(F32)).astype(BF16)
    return high, middle, low


def rms(values, scaling):
    floats = values.astype(F32)
    mean = jnp.mean(floats * floats, axis=-1, keepdims=True)
    return (floats * lax.rsqrt(mean + 1e-06) * scaling).astype(BF16)


def key_value_kernel(latent, scaling, key_up, value_up, rotary, out):
    tokens = latent.shape[0]
    context = rms(latent[...], scaling[...])
    both = jnp.concatenate([dot(context, key_up[...]), dot(context, value_up[...])], axis=1)
    out[0 : PLAIN + VALUE, :] = both.T.astype(BF16)
    wide = jnp.concatenate(
        [rotary[...].astype(F32), jnp.zeros((tokens, 128 - ROTARY), F32)], axis=1
    )
    out[PLAIN + VALUE :, :] = wide.T[0:ROTARY, :].astype(BF16)


def query_kernel(place, latent, scaling, plain, rotary, cos, sin, out):
    tokens = latent.shape[0]
    compressed = rms(latent[...], scaling[...])
    wide = jnp.concatenate(
        [
            dot(compressed, plain[...]),
            dot(compressed, rotary[...]),
            jnp.zeros((tokens, 128 - PLAIN - ROTARY), F32),
        ],
        axis=1,
    ).T
    half = ROTARY // 2
    a, b = wide[PLAIN : PLAIN + half, :], wide[PLAIN + half : PLAIN + ROTARY, :]
    c, s = cos[place[0]], sin[place[0]]
    high, middle, low = split3(jnp.concatenate([a * c - b * s, a * s + b * c], axis=0))
    out[...] = jnp.concatenate(
        [wide[0:PLAIN, :].astype(BF16), high, high, middle, middle, high, low], axis=0
    )


def attention_kernel(query, kv, shared, cos, sin, out, scores):
    blocks, _, width = kv.shape
    q = query[...].astype(F32).T.astype(BF16)
    half = ROTARY // 2
    scale = (PLAIN + ROTARY) ** -0.5
    tokens = q.shape[0]

    top = jnp.full((tokens, width), -jnp.inf, F32)
    for j in range(blocks):
        raw = kv[j, PLAIN + VALUE :, :].astype(F32)
        a, b = raw[0:half, :], raw[half:, :]
        c, s = cos[j], sin[j]
        high, middle, low = split3(jnp.concatenate([a * c - b * s, a * s + b * c], axis=0))
        keys = jnp.concatenate(
            [kv[j, 0:PLAIN, :], high, middle, high, middle, low, high], axis=0
        )
        part = dot(q, keys) * scale
        scores[:, j * width : (j + 1) * width] = part
        top = jnp.maximum(top, part)
    largest = jnp.max(top, axis=1, keepdims=True)
    total = jnp.zeros((tokens, width), F32)
    summed = jnp.zeros((VALUE, tokens), F32)
    for j in range(blocks):
        weights = jnp.exp(scores[:, j * width : (j + 1) * width] - largest)
        total = total + weights
        summed = summed + dot(kv[j, PLAIN : PLAIN + VALUE, :], weights.astype(BF16), 1, 1)
    whole = jnp.broadcast_to(jnp.sum(total, axis=1, keepdims=True), (tokens, width)).T
    heads = (summed / whole[0:VALUE, :]).astype(BF16)
    sent = jnp.concatenate([heads, shared[...]], axis=0)
    for t in range(out.shape[0]):
        out[t] = sent


def dispatch_kernel(place, rows, gain, routes, gate, up, sent, slots, shared, normed, *, experts, capacity):
    tokens = rows.shape[0]
    floats = rows[...].astype(F32)
    centred = floats - jnp.mean(floats, axis=-1, keepdims=True)
    variance = jnp.mean(centred * centred, axis=-1, keepdims=True)
    values = (centred * lax.rsqrt(variance + 1e-05) * gain[...]).astype(BF16)
    normed[...] = values
    lanes = lax.broadcasted_iota(jnp.int32, (tokens, 128), 1)
    chosen = [routes[:, k : k + 1] for k in range(routes.shape[1])]
    marks = [(lanes == c) for c in chosen]
    named = sum(jnp.where(m, 1.0, 0.0) for m in marks).astype(BF16)
    earlier = (
        lax.broadcasted_iota(jnp.int32, (tokens, tokens), 0)
        > lax.broadcasted_iota(jnp.int32, (tokens, tokens), 1)
    )
    before = dot(jnp.where(earlier, 1.0, 0.0).astype(BF16), named)
    places = lax.broadcasted_iota(jnp.int32, (tokens, experts * capacity), 1)
    hot = jnp.zeros((tokens, experts * capacity), F32)
    for k, (c, m) in enumerate(zip(chosen, marks)):
        rank = jnp.sum(jnp.where(m, before, 0.0), axis=1, keepdims=True).astype(jnp.int32)
        slot = c * capacity + rank
        slots[:, k : k + 1] = slot
        hot = jnp.where(places == slot, 1.0, hot)
    width = sent.shape[1]
    own = normed[:, pl.ds(pl.multiple_of(place[1] * width, width), width)]
    sent[...] = dot(hot.T.astype(BF16), own).astype(BF16)
    g = dot(values, gate[...])
    u = dot(values, up[...])
    hidden = g / (1.0 + jnp.exp(-g)) * u
    wide = jnp.concatenate(
        [hidden, jnp.zeros((tokens, 128 - hidden.shape[1]), F32)], axis=1
    )
    shared[...] = wide.T[0 : hidden.shape[1], :].astype(BF16)


def spread_kernel(order, rows, out):
    placed = dot(order[...], rows[...]).astype(BF16)
    half = out.shape[2]
    for c in range(out.shape[0]):
        part = placed[c * half : (c + 1) * half, :]
        for t in range(out.shape[1]):
            out[c, t] = part


def expert_kernel(rows, gate, up, down, out):
    parts, wide = rows.shape[0], rows.shape[1]
    width = out.shape[3]
    for c in range(parts):
        x = jnp.concatenate([rows[c, t] for t in range(wide)], axis=1)
        g = dot(x, gate[...])
        u = dot(x, up[...])
        hidden = (g / (1.0 + jnp.exp(-g)) * u).astype(BF16)
        for t in range(wide):
            out[c, t] = dot(hidden, down[t]).astype(BF16)


def gathered_sum_kernel(order, partial, out):
    parts, wide = partial.shape[0], partial.shape[1]
    sums = []
    for c in range(parts):
        total = partial[c, 0].astype(F32)
        for t in range(1, wide):
            total = total + partial[c, t].astype(F32)
        sums.append(total.astype(BF16))
    out[...] = dot(order[...], jnp.concatenate(sums, axis=0), 0, 0).astype(BF16)


def final_kernel(returned, slots, route_weight, both, output_weight, shared_down, attended, combined):
    tokens = slots.shape[0]
    places = lax.broadcasted_iota(jnp.int32, (tokens, returned.shape[0]), 1)
    routed = jnp.zeros((tokens, returned.shape[1]), F32)
    for k in range(slots.shape[1]):
        hot = jnp.where(places == slots[:, k : k + 1], 1.0, 0.0).astype(BF16)
        routed = routed + dot(hot, returned[...]) * route_weight[:, k : k + 1]
    heads = jnp.concatenate([both[t, 0:VALUE, :] for t in range(both.shape[0])], axis=0)
    hidden = jnp.concatenate([both[t, VALUE:, :] for t in range(both.shape[0])], axis=0)
    attended[...] = dot(heads, output_weight[...], 0, 0).astype(BF16)
    combined[...] = (dot(hidden, shared_down[...], 0, 0) + routed).astype(BF16)


def tables(positions, width):
    inverse = (1.0 / 10000.0 ** (np.arange(0, ROTARY, 2) / ROTARY)).astype(np.float32)
    angles = inverse[:, None] * np.arange(positions, dtype=np.float32)[None, :]
    angles = angles.astype(np.float64).reshape(ROTARY // 2, positions // width, width)
    angles = angles.transpose(1, 0, 2)
    return np.cos(angles).astype(np.float32), np.sin(angles).astype(np.float32)


def row_order(outer, inner, capacity):
    source = np.arange(outer * inner * capacity).reshape(outer, inner, capacity)
    source = source.transpose(1, 0, 2).reshape(-1)
    return np.eye(source.size, dtype=np.float32)[source]


def exchange(array, axes):
    return lax.all_to_all(array, axes, 0, 0, tiled=True)


def per_device(
    compressed_query,
    compressed_key_value,
    rotary_key,
    query_norm_scale,
    context_norm_scale,
    query_plain_weight,
    query_rotary_weight,
    key_up_weight,
    value_up_weight,
    output_weight,
    mixture_input,
    mixture_gain,
    routes,
    route_weight,
    expert_gate,
    expert_up,
    expert_down,
    shared_gate,
    shared_up,
    shared_down,
):
    tokens, model = mixture_input.shape
    planes, cores = lax.axis_size("z"), lax.axis_size("core")
    wide = lax.axis_size(TP)
    experts = planes * cores
    width = model // wide
    capacity = tokens * routes.shape[1] * 3 // (2 * experts)
    units = expert_gate.shape[2]
    shared_units = shared_gate.shape[1]
    place = jnp.stack([lax.axis_index(EP), lax.axis_index(TP)]).astype(jnp.int32)
    cos, sin = tables(tokens * experts, tokens)
    order = jnp.asarray(row_order(planes, cores, capacity), BF16)

    down = exchange(expert_down[0].reshape(wide, units, width), TP)

    kv = call(
        key_value_kernel,
        shape((PLAIN + VALUE + ROTARY, tokens)),
        (compressed_key_value, context_norm_scale[None], key_up_weight, value_up_weight, rotary_key),
    )
    all_kv = lax.all_gather(kv, EP, axis=0, tiled=True).reshape(experts, *kv.shape)

    sent, slots, shared, _ = call(
        functools.partial(dispatch_kernel, experts=experts, capacity=capacity),
        (
            shape((experts * capacity, width)),
            shape((tokens, routes.shape[1]), jnp.int32),
            shape((shared_units, tokens)),
            shape((tokens, model)),
        ),
        (place, mixture_input, mixture_gain[None], routes, shared_gate, shared_up),
        smem=1,
    )
    query = call(
        query_kernel,
        shape((PLAIN + 6 * ROTARY, tokens)),
        (
            place,
            compressed_query,
            query_norm_scale[None],
            query_plain_weight,
            query_rotary_weight,
            cos,
            sin,
        ),
        smem=1,
    )

    moved = exchange(sent.reshape(planes, cores * capacity, width), "z")
    rows = planes * capacity
    spread = call(
        spread_kernel,
        shape((cores, wide, rows, width)),
        (order, moved.reshape(experts * capacity, width)),
    )
    arrived = exchange(spread.reshape(cores * wide, rows, width), PLANE)
    partial = call(
        expert_kernel,
        shape((cores, wide, rows, width)),
        (arrived.reshape(cores, wide, rows, width), expert_gate[0], expert_up[0], down),
    )
    parts = exchange(partial.reshape(cores * wide, rows, width), PLANE)
    summed = call(
        gathered_sum_kernel,
        shape((experts * capacity, width)),
        (order, parts.reshape(cores, wide, rows, width)),
    )
    returned = exchange(summed.reshape(planes, cores * capacity, width), "z")

    both = pl.pallas_call(
        attention_kernel,
        out_shape=shape((wide, VALUE + shared_units, tokens)),
        in_specs=[VMEM] * 5,
        out_specs=VMEM,
        scratch_shapes=[pltpu.VMEM((tokens, tokens * experts), F32)],
        cost_estimate=pl.CostEstimate(flops=10**9, bytes_accessed=10**6, transcendentals=0),
    )(query, all_kv, shared, cos, sin)
    both = exchange(both, TP)
    return call(
        final_kernel,
        (shape((tokens, width)), shape((tokens, width))),
        (
            returned.reshape(experts * capacity, width),
            slots,
            route_weight,
            both,
            output_weight,
            shared_down,
        ),
    )


def solution(mesh):
    split = Mesh(mesh.devices.reshape(16, 2, 4, 4), ("z", "core", "y", "x"))
    placed = (
        P(EP, None),
        P(EP, None),
        P(EP, None),
        P(),
        P(),
        P(None, TP),
        P(None, TP),
        P(None, TP),
        P(None, TP),
        P(None, TP),
        P(EP, None),
        P(),
        P(EP, None),
        P(EP, None),
        P(EP, None, TP),
        P(EP, None, TP),
        P(EP, None, TP),
        P(None, TP),
        P(None, TP),
        P(None, TP),
    )
    return jax.shard_map(
        per_device,
        mesh=split,
        in_specs=placed,
        out_specs=(P(EP, TP), P(EP, TP)),
        check_vma=False,
    )
```

time: 205 us -> 196 us (0.956)
  blocking collectives: 54.7 us -> 28.3 us
  Pallas kernels: 0 us -> 25.6 us
  matrix products: 15.2 us -> 0 us
  waiting for transfers between devices: 67.5 us -> 82.1 us
  other arithmetic: 8.19 us -> 0.61 us
  starting transfers between devices: 23.8 us -> 30.5 us
  local copies, waits for them, and re-layouts: 19.8 us -> 13.5 us
    all_to_all x3 -> x5, waiting for transfers between devices: 21.7 us -> 51.4 us  [exchange(): return lax.all_to_all(array, axes, 0, 0, tiled=True)]
    pallas_call x0 -> x8, Pallas kernels: none -> 25.6 us  [the longest x7 20.6 us: call(): pl.pallas_call(body, out_shape=outs, in_specs=[SMEM] * smem + [VMEM] * (l...]
    all_gather x1 -> x0, blocking collectives: 23.1 us -> none  [per_device(): lax.all_gather(shared_hidden, 'tp', axis=1, tiled=True)]
    dot_general x17 -> x0, matrix products: 15.2 us -> none  [the longest x2 3.62 us: attend(): jnp.einsum('qhr,kr->hqk', query_rot, turned, precision=lax.Precision.HIGH...]
    all_gather x2 -> x1, waiting for transfers between devices: 45.7 us -> 30.8 us  [per_device(): lax.all_gather(kv, EP, axis=0, tiled=True).reshape(experts, *kv.shape)]
    unnamed x33, local copies, waits for them, and re-layouts: 2.31 us -> 12.9 us
    all_to_all x3 -> x5, starting transfers between devices: 23.7 us -> 30.5 us  [exchange(): return lax.all_to_all(array, axes, 0, 0, tiled=True)]
    reshape x3 -> x0, local copies, waits for them, and re-layouts: 4.31 us -> none  [the longest x1 3.6 us: per_device(): outgoing = padded[owners].reshape(experts, capacity, model_width)]
  transfers between devices with their start and end apart: 5 -> 6, of which waited for: 2 -> 5; matrix products, arithmetic and copies ran while one was open for 18% -> 3% of each run, Pallas kernels for 0% -> 10%
where the time goes in v1:
time: 196 us; the launch traced here: 195 us
  waiting for transfers between devices  82.1 us (42%)
  starting transfers between devices  30.5 us (16%)
  blocking collectives  28.3 us (14%)
  Pallas kernels  25.6 us (13%)
  between operations  14.1 us (7%)
  local copies, waits for them, and re-layouts  13.5 us (7%)
    all_to_all x5, waiting for transfers between devices, exchange(): return lax.all_to_all(array, axes, 0, 0, tiled=True)  51.4 us
    all_gather x1, waiting for transfers between devices, per_device(): lax.all_gather(kv, EP, axis=0, tiled=True).reshape(experts, *kv.shape)  30.8 us
    all_to_all x5, starting transfers between devices, exchange(): return lax.all_to_all(array, axes, 0, 0, tiled=True)  30.5 us
    all_to_all x1, blocking collectives, exchange(): return lax.all_to_all(array, axes, 0, 0, tiled=True)  28.3 us
    pallas_call x7, Pallas kernels, call(): pl.pallas_call(body, out_shape=outs, in_specs=[SMEM] * smem + [VMEM] * (l...  20.6 us
    unnamed x33, local copies, waits for them, and re-layouts  12.9 us
    pallas_call x1, Pallas kernels, per_device(): pl.pallas_call(attention_kernel, out_shape=shape((wide, VALUE + shared_un...  4.99 us
  transfers between devices with their start and end apart: 6, of which 5 were waited for; matrix products, arithmetic and copies ran while one was open for 3% of the time, Pallas kernels for 10%

profile of v1, /device:TPU:32, one launch (start us, length us, event | category | flops | bytes accessed | tf_op | source)
XLA Modules:
  0.0 194.7 jit_solution(3842496078635467529)
XLA Ops:
  7.2 1.4 copy.25.routes
  8.6 1.9 copy.26.gate
  10.5 1.9 copy.27.up
  12.4 0.6 pad_add_fusion.place
  13.0 3.1 %shard_map.230 = (bf16[384,128]{1,0:T(8,128)(2,1)}, s32[128,2]{1,0:T(8,128)}, bf16[32,128]{1,0:T(8,128)(2,1)}, bf16[128,2048]{1,0:T(8,128)(2,1)}) custom-call(s32[2]{0:T(128)} %pad_add_fusion.place, bf16[128,2048]{1,0:T(8,128)(2,1)} %rows.1, f32[1,2048]{1,0:T(1,128)} %bitcast.27, s32[128,2]{1,0:T(8,128)} %copy.25.routes, bf16[2048,32]{1,0:T(8,128)(2,1)} %copy.26.gate, ...), custom_call_target="tpu_custom_call" | custom-call | flops 1000000000 | bytes 1000000 | tf_op jit(solution)/shard_map/pallas_call | solution.py:29
  16.1 28.3 %all_to_all.30 = bf16[16,24,128]{2,1,0:T(8,128)(2,1)} all-to-all(bf16[16,24,128]{2,1,0:T(8,128)(2,1)} %bitcast.24), channel_id=1, replica_groups=mesh['z'=16,'core'=2,'y'=4,'x'=4] {'z'}, dimensions={0} | all-to-all | bytes 196608 | tf_op jit(solution)/shard_map/all_to_all | solution.py:217
  44.4 7.0 %all-to-all-start.2 = ((bf16[16,256,128]{2,1,0:T(8,128)(2,1)}), bf16[16,256,128]{2,1,0:T(8,128)(2,1)S(1)}, u32[]{:S(2)}, u32[]{:S(2)}) async-start(bf16[16,256,128]{2,1,0:T(8,128)(2,1)} %bitcast.9), calls=%async_computation.2 | async-start | bytes 2097152 | tf_op jit(solution)/shard_map/all_to_all | solution.py:217
  51.4 2.5 %shard_map.231 = bf16[2,16,192,128]{3,2,1,0:T(8,128)(2,1)} custom-call(bf16[384,384]{1,0:T(8,128)(2,1)} %constant.28.clone.order, bf16[384,128]{1,0:T(8,128)(2,1)} %bitcast.25), custom_call_target="tpu_custom_call" | custom-call | flops 1000000000 | bytes 1000000 | tf_op jit(solution)/shard_map/pallas_call | solution.py:29
  53.9 13.0 %all-to-all-done.2.down = bf16[16,256,128]{2,1,0:T(8,128)(2,1)S(1)} async-done(((bf16[16,256,128]{2,1,0:T(8,128)(2,1)}), bf16[16,256,128]{2,1,0:T(8,128)(2,1)S(1)}, u32[]{:S(2)}, u32[]{:S(2)}) %all-to-all-start.2) | async-done | bytes 1048608 | tf_op jit(solution)/shard_map/all_to_all | solution.py:217
  66.9 1.0 copy-done.1
  67.9 4.0 %all-to-all-start.1 = ((bf16[32,192,128]{2,1,0:T(8,128)(2,1)}), bf16[32,192,128]{2,1,0:T(8,128)(2,1)S(1)}, u32[]{:S(2)}, u32[]{:S(2)}) async-start(bf16[32,192,128]{2,1,0:T(8,128)(2,1)} %bitcast.19), calls=%async_computation.1 | async-start | bytes 3145728 | tf_op jit(solution)/shard_map/all_to_all | solution.py:217
  71.9 0.7 copy.30.key_up
  72.7 0.8 copy.31.value_up
  73.5 0.7 copy.32.rotary
  74.2 2.1 %shard_map.235 = bf16[160,128]{1,0:T(8,128)(2,1)} custom-call(bf16[128,512]{1,0:T(8,128)(2,1)} %latent.3, f32[1,512]{1,0:T(1,128)} %bitcast.28, bf16[512,64]{1,0:T(8,128)(2,1)} %copy.30.key_up, bf16[512,64]{1,0:T(8,128)(2,1)} %copy.31.value_up, bf16[128,32]{1,0:T(8,128)(2,1)} %copy.32.rotary), custom_call_target="tpu_custom_call" | custom-call | flops 1000000000 | bytes 1000000 | tf_op jit(solution)/shard_map/pallas_call | solution.py:29
  76.3 19.0 %all-to-all-done.1 = bf16[32,192,128]{2,1,0:T(8,128)(2,1)S(1)} async-done(((bf16[32,192,128]{2,1,0:T(8,128)(2,1)}), bf16[32,192,128]{2,1,0:T(8,128)(2,1)S(1)}, u32[]{:S(2)}, u32[]{:S(2)}) %all-to-all-start.1) | async-done | bytes 1572896 | tf_op jit(solution)/shard_map/all_to_all | solution.py:217
  95.3 1.1 copy-done
  96.4 5.5 %shard_map.232 = bf16[2,16,192,128]{3,2,1,0:T(8,128)(2,1)} custom-call(bf16[2,16,192,128]{3,2,1,0:T(8,128)(2,1)} %bitcast.16, bf16[2048,256]{1,0:T(8,128)(2,1)} %bitcast.20, bf16[2048,256]{1,0:T(8,128)(2,1)} %bitcast.21, bf16[16,256,128]{2,1,0:T(8,128)(2,1)} %copy-done.1), custom_call_target="tpu_custom_call" | custom-call | flops 1000000000 | bytes 1000000 | tf_op jit(solution)/shard_map/pallas_call | solution.py:29
  101.9 4.1 %all-to-all-start.3 = ((bf16[32,192,128]{2,1,0:T(8,128)(2,1)}), bf16[32,192,128]{2,1,0:T(8,128)(2,1)S(1)}, u32[]{:S(2)}, u32[]{:S(2)}) async-start(bf16[32,192,128]{2,1,0:T(8,128)(2,1)} %bitcast.17), calls=%async_computation.3 | async-start | bytes 3145728 | tf_op jit(solution)/shard_map/all_to_all | solution.py:217
  106.7 1.0 copy.28.plain
  107.6 0.9 copy.29.rotary
  108.6 2.6 %shard_map.234.query = bf16[256,128]{1,0:T(8,128)(2,1)} custom-call(s32[2]{0:T(128)} %pad_add_fusion.place, bf16[128,1536]{1,0:T(8,128)(2,1)} %latent.2, f32[1,1536]{1,0:T(1,128)} %broadcast_in_dim.10.scaling, bf16[1536,64]{1,0:T(8,128)(2,1)} %copy.28.plain, bf16[1536,32]{1,0:T(8,128)(2,1)} %copy.29.rotary, f32[32,16,128]{2,1,0:T(8,128)} %constant.29.clone.cos, ...), custom_call_target="tpu_custom_call" | custom-call | flops 1000000000 | bytes 1000000 | tf_op jit(solution)/shard_map/pallas_call | solution.py:29
  111.2 30.8 %all-gather.2.cloned.1.call-done = bf16[5120,128]{1,0:T(8,128)(2,1)} async-done(((bf16[160,128]{1,0:T(8,128)(2,1)}), bf16[5120,128]{1,0:T(8,128)(2,1)}) %all-gather.2.cloned.1.call-update) | async-done | bytes 1310736 | tf_op jit(solution)/shard_map/all_gather | solution.py:261
  142.0 5.0 %shard_map.236 = bf16[16,96,128]{2,1,0:T(8,128)(2,1)} custom-call(bf16[256,128]{1,0:T(8,128)(2,1)} %shard_map.234.query, bf16[32,160,128]{2,1,0:T(8,128)(2,1)} %bitcast.26, bf16[32,128]{1,0:T(8,128)(2,1)} %get-tuple-element.7.shared, f32[32,16,128]{2,1,0:T(8,128)} %constant.29.clone.cos, f32[32,16,128]{2,1,0:T(8,128)} %constant.30.clone.sin), custom_call_target="tpu_custom_call" | custom-call | flops 1000000000 | bytes 1000000 | tf_op jit(solution)/shard_map/pallas_call | solution.py:310
  147.0 6.7 %all-to-all-start.5 = ((bf16[16,96,128]{2,1,0:T(8,128)(2,1)}), bf16[16,96,128]{2,1,0:T(8,128)(2,1)S(1)}, u32[]{:S(2)}, u32[]{:S(2)}) async-start(bf16[16,96,128]{2,1,0:T(8,128)(2,1)} %shard_map.236), calls=%async_computation.5 | async-start | bytes 786432 | tf_op jit(solution)/shard_map/all_to_all | solution.py:217
  153.7 2.5 %shard_map.233 = bf16[384,128]{1,0:T(8,128)(2,1)} custom-call(bf16[384,384]{1,0:T(8,128)(2,1)} %constant.28.clone.order, bf16[2,16,192,128]{3,2,1,0:T(8,128)(2,1)} %bitcast.18), custom_call_target="tpu_custom_call" | custom-call | flops 1000000000 | bytes 1000000 | tf_op jit(solution)/shard_map/pallas_call | solution.py:29
  156.2 7.9 %all-to-all-done.5.both = bf16[16,96,128]{2,1,0:T(8,128)(2,1)S(1)} async-done(((bf16[16,96,128]{2,1,0:T(8,128)(2,1)}), bf16[16,96,128]{2,1,0:T(8,128)(2,1)S(1)}, u32[]{:S(2)}, u32[]{:S(2)}) %all-to-all-start.5) | async-done | bytes 393248 | tf_op jit(solution)/shard_map/all_to_all | solution.py:217
  164.1 8.7 %all-to-all-start.4 = ((bf16[16,24,128]{2,1,0:T(8,128)(2,1)}), bf16[16,24,128]{2,1,0:T(8,128)(2,1)S(1)}, u32[]{:S(2)}, u32[]{:S(2)}) async-start(bf16[16,24,128]{2,1,0:T(8,128)(2,1)} %bitcast.23), calls=%async_computation.4 | async-start | bytes 196608 | tf_op jit(solution)/shard_map/all_to_all | solution.py:217
  172.8 0.7 copy.33.route_weight
  173.5 11.5 %all-to-all-done.4 = bf16[16,24,128]{2,1,0:T(8,128)(2,1)S(1)} async-done(((bf16[16,24,128]{2,1,0:T(8,128)(2,1)}), bf16[16,24,128]{2,1,0:T(8,128)(2,1)S(1)}, u32[]{:S(2)}, u32[]{:S(2)}) %all-to-all-start.4) | async-done | bytes 98336 | tf_op jit(solution)/shard_map/all_to_all | solution.py:217
  185.1 0.6 copy-done.5
  185.7 2.2 %shard_map.237 = (bf16[128,128]{1,0:T(8,128)(2,1)}, bf16[128,128]{1,0:T(8,128)(2,1)}) custom-call(bf16[384,128]{1,0:T(8,128)(2,1)} %bitcast.22, s32[128,2]{1,0:T(8,128)} %get-tuple-element.6.slots, f32[128,2]{1,0:T(8,128)} %copy.33.route_weight, bf16[16,96,128]{2,1,0:T(8,128)(2,1)} %copy-done.3, bf16[1024,128]{1,0:T(8,128)(2,1)} %output_weight.1, ...), custom_call_target="tpu_custom_call" | custom-call | flops 1000000000 | bytes 1000000 | tf_op jit(solution)/shard_map/pallas_call | solution.py:29
  (25 shorter events, 0.7 us)
Async XLA Ops:
  44.4 22.5 %all-to-all-start.2 = ((bf16[16,256,128]{2,1,0:T(8,128)(2,1)}), bf16[16,256,128]{2,1,0:T(8,128)(2,1)S(1)}, u32[]{:S(2)}, u32[]{:S(2)}) async-start(bf16[16,256,128]{2,1,0:T(8,128)(2,1)} %bitcast.9), calls=%async_computation.2 | async-start | bytes 2097152 | tf_op jit(solution)/shard_map/all_to_all | solution.py:217
  66.9 1.0 copy-start.1
  66.9 5.0 %copy-start.7 = (bf16[512,64]{0,1:T(8,128)(2,1)S(1)}, bf16[512,64]{0,1:T(8,128)(2,1)}, u32[]{:S(2)}) copy-start(bf16[512,64]{0,1:T(8,128)(2,1)} %param.30) | copy-start | bytes 196612
  66.9 5.8 %copy-start.8 = (bf16[512,64]{0,1:T(8,128)(2,1)S(1)}, bf16[512,64]{0,1:T(8,128)(2,1)}, u32[]{:S(2)}) copy-start(bf16[512,64]{0,1:T(8,128)(2,1)} %param.31) | copy-start | bytes 196612
  66.9 6.6 %copy-start.9 = (bf16[128,32]{0,1:T(8,128)(2,1)S(1)}, bf16[128,32]{0,1:T(8,128)(2,1)}, u32[]{:S(2)}) copy-start(bf16[128,32]{0,1:T(8,128)(2,1)} %param.25) | copy-start | bytes 24580
  67.9 27.4 %all-to-all-start.1 = ((bf16[32,192,128]{2,1,0:T(8,128)(2,1)}), bf16[32,192,128]{2,1,0:T(8,128)(2,1)S(1)}, u32[]{:S(2)}, u32[]{:S(2)}) async-start(bf16[32,192,128]{2,1,0:T(8,128)(2,1)} %bitcast.19), calls=%async_computation.1 | async-start | bytes 3145728 | tf_op jit(solution)/shard_map/all_to_all | solution.py:217
  71.9 70.1 %all-gather.2.cloned.1.call-start = ((), (), s32[]{:S(2)}) async-start(), calls=%async_computation.6 | async-start | bytes 1351680 | tf_op jit(solution)/shard_map/all_gather | solution.py:261
  95.3 1.1 copy-start
  101.9 4.1 %copy-start.10 = (f32[1536]{0:T(1024)S(1)}, f32[1536]{0:T(1024)}, u32[]{:S(2)}) copy-start(f32[1536]{0:T(1024)} %param.26) | copy-start | bytes 18436
  101.9 4.7 %copy-start.4 = (bf16[1536,64]{0,1:T(8,128)(2,1)S(1)}, bf16[1536,64]{0,1:T(8,128)(2,1)}, u32[]{:S(2)}) copy-start(bf16[1536,64]{0,1:T(8,128)(2,1)} %param.28) | copy-start | bytes 589828
  101.9 5.7 %copy-start.6 = (bf16[1536,32]{0,1:T(8,128)(2,1)S(1)}, bf16[1536,32]{0,1:T(8,128)(2,1)}, u32[]{:S(2)}) copy-start(bf16[1536,32]{0,1:T(8,128)(2,1)} %param.29) | copy-start | bytes 294916
  101.9 45.0 %all-to-all-start.3 = ((bf16[32,192,128]{2,1,0:T(8,128)(2,1)}), bf16[32,192,128]{2,1,0:T(8,128)(2,1)S(1)}, u32[]{:S(2)}, u32[]{:S(2)}) async-start(bf16[32,192,128]{2,1,0:T(8,128)(2,1)} %bitcast.17), calls=%async_computation.3 | async-start | bytes 3145728 | tf_op jit(solution)/shard_map/all_to_all | solution.py:217
  147.0 6.7 %copy-start.2 = (bf16[32,192,128]{2,1,0:T(8,128)(2,1)}, bf16[32,192,128]{2,1,0:T(8,128)(2,1)S(1)}, u32[]{:S(2)}) copy-start(bf16[32,192,128]{2,1,0:T(8,128)(2,1)S(1)} %all-to-all-done.3) | copy-start | bytes 4718596
  147.0 17.1 %all-to-all-start.5 = ((bf16[16,96,128]{2,1,0:T(8,128)(2,1)}), bf16[16,96,128]{2,1,0:T(8,128)(2,1)S(1)}, u32[]{:S(2)}, u32[]{:S(2)}) async-start(bf16[16,96,128]{2,1,0:T(8,128)(2,1)} %shard_map.236), calls=%async_computation.5 | async-start | bytes 786432 | tf_op jit(solution)/shard_map/all_to_all | solution.py:217
  153.7 19.2 %copy-start.11 = (f32[128,2]{0,1:T(2,128)S(1)}, f32[128,2]{0,1:T(2,128)}, u32[]{:S(2)}) copy-start(f32[128,2]{0,1:T(2,128)} %param.36) | copy-start | bytes 3076
  164.1 20.9 %copy-start.3 = (bf16[16,96,128]{2,1,0:T(8,128)(2,1)}, bf16[16,96,128]{2,1,0:T(8,128)(2,1)S(1)}, u32[]{:S(2)}) copy-start(bf16[16,96,128]{2,1,0:T(8,128)(2,1)S(1)} %all-to-all-done.5.both) | copy-start | bytes 1179652
  164.1 20.9 %all-to-all-start.4 = ((bf16[16,24,128]{2,1,0:T(8,128)(2,1)}), bf16[16,24,128]{2,1,0:T(8,128)(2,1)S(1)}, u32[]{:S(2)}, u32[]{:S(2)}) async-start(bf16[16,24,128]{2,1,0:T(8,128)(2,1)} %bitcast.23), calls=%async_computation.4 | async-start | bytes 196608 | tf_op jit(solution)/shard_map/all_to_all | solution.py:217
  185.0 0.6 copy-start.5
Sparse Core Ops, SparseCore 0:
  76.4 65.5 all-gather.1

commit v2 on v1

--- a/solution.py
+++ b/solution.py
@@ -25,15 +25,15 @@
     return lax.dot_general(a, b, (((ca,), (cb,)), ((), ())), preferred_element_type=F32)
 
 
-def call(body, outs, args, smem=0, flops=10**9, bytes_accessed=10**6):
+def call(body, outs, args, smem=0, scratch=(), limit=8):
     return pl.pallas_call(
         body,
         out_shape=outs,
         in_specs=[SMEM] * smem + [VMEM] * (len(args) - smem),
         out_specs=jax.tree.map(lambda _: VMEM, outs),
-        cost_estimate=pl.CostEstimate(
-            flops=flops, bytes_accessed=bytes_accessed, transcendentals=0
-        ),
+        scratch_shapes=scratch,
+        compiler_params=pltpu.CompilerParams(vmem_limit_bytes=limit << 20),
+        cost_estimate=pl.CostEstimate(flops=10**9, bytes_accessed=10**6, transcendentals=0),
     )(*args)
 
 
@@ -56,60 +56,51 @@
 
 
 def key_value_kernel(latent, scaling, key_up, value_up, rotary, out):
-    tokens = latent.shape[0]
     context = rms(latent[...], scaling[...])
-    both = jnp.concatenate([dot(context, key_up[...]), dot(context, value_up[...])], axis=1)
-    out[0 : PLAIN + VALUE, :] = both.T.astype(BF16)
-    wide = jnp.concatenate(
-        [rotary[...].astype(F32), jnp.zeros((tokens, 128 - ROTARY), F32)], axis=1
-    )
-    out[PLAIN + VALUE :, :] = wide.T[0:ROTARY, :].astype(BF16)
+    out[0:PLAIN, :] = dot(key_up[...], context, 1, 1).astype(BF16)
+    out[PLAIN : PLAIN + VALUE, :] = dot(value_up[...], context, 1, 1).astype(BF16)
+    out[PLAIN + VALUE :, :] = rotary[...]
 
 
 def query_kernel(place, latent, scaling, plain, rotary, cos, sin, out):
-    tokens = latent.shape[0]
     compressed = rms(latent[...], scaling[...])
-    wide = jnp.concatenate(
-        [
-            dot(compressed, plain[...]),
-            dot(compressed, rotary[...]),
-            jnp.zeros((tokens, 128 - PLAIN - ROTARY), F32),
-        ],
-        axis=1,
-    ).T
+    nope = dot(plain[...], compressed, 1, 1).astype(BF16)
+    turn = dot(rotary[...], compressed, 1, 1)
     half = ROTARY // 2
-    a, b = wide[PLAIN : PLAIN + half, :], wide[PLAIN + half : PLAIN + ROTARY, :]
+    a, b = turn[0:half, :], turn[half:, :]
     c, s = cos[place[0]], sin[place[0]]
     high, middle, low = split3(jnp.concatenate([a * c - b * s, a * s + b * c], axis=0))
-    out[...] = jnp.concatenate(
-        [wide[0:PLAIN, :].astype(BF16), high, high, middle, middle, high, low], axis=0
-    )
-
-
-def attention_kernel(query, kv, shared, cos, sin, out, scores):
-    blocks, _, width = kv.shape
-    q = query[...].astype(F32).T.astype(BF16)
+    whole = jnp.concatenate([nope, high, high, middle, middle, high, low], axis=0)
+    out[...] = whole.astype(F32).T.astype(BF16)
+
+
+def attention_kernel(place, query, mine, other, shared, cos, sin, out, scores, *, order):
+    q = query[...]
+    planes, _, width = mine.shape
     half = ROTARY // 2
     scale = (PLAIN + ROTARY) ** -0.5
     tokens = q.shape[0]
+    blocks = [(kv, j) for kv in (mine, other) for j in range(planes)]
 
     top = jnp.full((tokens, width), -jnp.inf, F32)
-    for j in range(blocks):
+    for n, (kv, j) in enumerate(blocks):
+        core = place[2] if kv is mine else 1 - place[2]
+        at = ((place[1] + (planes - order[j])) % planes) * 2 + core
         raw = kv[j, PLAIN + VALUE :, :].astype(F32)
         a, b = raw[0:half, :], raw[half:, :]
-        c, s = cos[j], sin[j]
+        c, s = cos[at], sin[at]
         high, middle, low = split3(jnp.concatenate([a * c - b * s, a * s + b * c], axis=0))
         keys = jnp.concatenate(
             [kv[j, 0:PLAIN, :], high, middle, high, middle, low, high], axis=0
         )
         part = dot(q, keys) * scale
-        scores[:, j * width : (j + 1) * width] = part
+        scores[:, n * width : (n + 1) * width] = part
         top = jnp.maximum(top, part)
     largest = jnp.max(top, axis=1, keepdims=True)
     total = jnp.zeros((tokens, width), F32)
     summed = jnp.zeros((VALUE, tokens), F32)
-    for j in range(blocks):
-        weights = jnp.exp(scores[:, j * width : (j + 1) * width] - largest)
+    for n, (kv, j) in enumerate(blocks):
+        weights = jnp.exp(scores[:, n * width : (n + 1) * width] - largest)
         total = total + weights
         summed = summed + dot(kv[j, PLAIN : PLAIN + VALUE, :], weights.astype(BF16), 1, 1)
     whole = jnp.broadcast_to(jnp.sum(total, axis=1, keepdims=True), (tokens, width)).T
@@ -119,6 +110,11 @@
         out[t] = sent
 
 
+def one_hot(slots, k, rows):
+    places = lax.broadcasted_iota(jnp.int32, (rows, slots.shape[1]), 0)
+    return jnp.where(places == slots[k : k + 1, :], 1.0, 0.0)
+
+
 def dispatch_kernel(place, rows, gain, routes, gate, up, sent, slots, shared, normed, *, experts, capacity):
     tokens = rows.shape[0]
     floats = rows[...].astype(F32)
@@ -126,32 +122,24 @@
     variance = jnp.mean(centred * centred, axis=-1, keepdims=True)
     values = (centred * lax.rsqrt(variance + 1e-05) * gain[...]).astype(BF16)
     normed[...] = values
-    lanes = lax.broadcasted_iota(jnp.int32, (tokens, 128), 1)
-    chosen = [routes[:, k : k + 1] for k in range(routes.shape[1])]
-    marks = [(lanes == c) for c in chosen]
-    named = sum(jnp.where(m, 1.0, 0.0) for m in marks).astype(BF16)
+    marks = [one_hot(routes, k, experts) for k in range(routes.shape[0])]
     earlier = (
         lax.broadcasted_iota(jnp.int32, (tokens, tokens), 0)
-        > lax.broadcasted_iota(jnp.int32, (tokens, tokens), 1)
-    )
-    before = dot(jnp.where(earlier, 1.0, 0.0).astype(BF16), named)
-    places = lax.broadcasted_iota(jnp.int32, (tokens, experts * capacity), 1)
-    hot = jnp.zeros((tokens, experts * capacity), F32)
-    for k, (c, m) in enumerate(zip(chosen, marks)):
-        rank = jnp.sum(jnp.where(m, before, 0.0), axis=1, keepdims=True).astype(jnp.int32)
-        slot = c * capacity + rank
-        slots[:, k : k + 1] = slot
-        hot = jnp.where(places == slot, 1.0, hot)
+        < lax.broadcasted_iota(jnp.int32, (tokens, tokens), 1)
+    )
+    before = dot(sum(marks).astype(BF16), jnp.where(earlier, 1.0, 0.0).astype(BF16))
+    for k, mark in enumerate(marks):
+        rank = jnp.sum(mark * before, axis=0, keepdims=True).astype(jnp.int32)
+        slots[k : k + 1, :] = routes[k : k + 1, :] * capacity + rank
+    hot = one_hot(slots, 0, experts * capacity)
+    for k in range(1, routes.shape[0]):
+        hot = hot + one_hot(slots, k, experts * capacity)
     width = sent.shape[1]
-    own = normed[:, pl.ds(pl.multiple_of(place[1] * width, width), width)]
-    sent[...] = dot(hot.T.astype(BF16), own).astype(BF16)
-    g = dot(values, gate[...])
-    u = dot(values, up[...])
-    hidden = g / (1.0 + jnp.exp(-g)) * u
-    wide = jnp.concatenate(
-        [hidden, jnp.zeros((tokens, 128 - hidden.shape[1]), F32)], axis=1
-    )
-    shared[...] = wide.T[0 : hidden.shape[1], :].astype(BF16)
+    own = normed[:, pl.ds(pl.multiple_of(place[3] * width, width), width)]
+    sent[...] = dot(hot.astype(BF16), own).astype(BF16)
+    g = dot(gate[...], values, 1, 1)
+    u = dot(up[...], values, 1, 1)
+    shared[...] = (g / (1.0 + jnp.exp(-g)) * u).astype(BF16)
 
 
 def spread_kernel(order, rows, out):
@@ -165,7 +153,6 @@
 
 def expert_kernel(rows, gate, up, down, out):
     parts, wide = rows.shape[0], rows.shape[1]
-    width = out.shape[3]
     for c in range(parts):
         x = jnp.concatenate([rows[c, t] for t in range(wide)], axis=1)
         g = dot(x, gate[...])
@@ -187,12 +174,12 @@
 
 
 def final_kernel(returned, slots, route_weight, both, output_weight, shared_down, attended, combined):
-    tokens = slots.shape[0]
-    places = lax.broadcasted_iota(jnp.int32, (tokens, returned.shape[0]), 1)
-    routed = jnp.zeros((tokens, returned.shape[1]), F32)
-    for k in range(slots.shape[1]):
-        hot = jnp.where(places == slots[:, k : k + 1], 1.0, 0.0).astype(BF16)
-        routed = routed + dot(hot, returned[...]) * route_weight[:, k : k + 1]
+    tokens, width = slots.shape[1], returned.shape[1]
+    routed = jnp.zeros((tokens, width), F32)
+    for k in range(slots.shape[0]):
+        hot = one_hot(slots, k, returned.shape[0]).astype(BF16)
+        scale = jnp.broadcast_to(route_weight[k : k + 1, :], (width, tokens)).T
+        routed = routed + dot(hot, returned[...], 0, 0) * scale
     heads = jnp.concatenate([both[t, 0:VALUE, :] for t in range(both.shape[0])], axis=0)
     hidden = jnp.concatenate([both[t, VALUE:, :] for t in range(both.shape[0])], axis=0)
     attended[...] = dot(heads, output_weight[...], 0, 0).astype(BF16)
@@ -247,7 +234,9 @@
     capacity = tokens * routes.shape[1] * 3 // (2 * experts)
     units = expert_gate.shape[2]
     shared_units = shared_gate.shape[1]
-    place = jnp.stack([lax.axis_index(EP), lax.axis_index(TP)]).astype(jnp.int32)
+    place = jnp.stack(
+        [lax.axis_index(EP), lax.axis_index("z"), lax.axis_index("core"), lax.axis_index(TP)]
+    ).astype(jnp.int32)
     cos, sin = tables(tokens * experts, tokens)
     order = jnp.asarray(row_order(planes, cores, capacity), BF16)
 
@@ -256,30 +245,44 @@
     kv = call(
         key_value_kernel,
         shape((PLAIN + VALUE + ROTARY, tokens)),
-        (compressed_key_value, context_norm_scale[None], key_up_weight, value_up_weight, rotary_key),
-    )
-    all_kv = lax.all_gather(kv, EP, axis=0, tiled=True).reshape(experts, *kv.shape)
+        (
+            compressed_key_value,
+            context_norm_scale[None],
+            key_up_weight.T,
+            value_up_weight.T,
+            rotary_key.T,
+        ),
+    )
+    mine, behind, step = kv[None], [0], planes // 2
+    while step:
+        ring = [(z, (z + step) % planes) for z in range(planes)]
+        received = lax.ppermute(mine, "z", ring)
+        mine = jnp.concatenate([mine, received], axis=0)
+        behind = behind + [(b + step) % planes for b in behind]
+        step //= 2
+    other = lax.ppermute(mine, "core", [(0, 1), (1, 0)])
 
     sent, slots, shared, _ = call(
         functools.partial(dispatch_kernel, experts=experts, capacity=capacity),
         (
             shape((experts * capacity, width)),
-            shape((tokens, routes.shape[1]), jnp.int32),
+            shape((routes.shape[1], tokens), jnp.int32),
             shape((shared_units, tokens)),
             shape((tokens, model)),
         ),
-        (place, mixture_input, mixture_gain[None], routes, shared_gate, shared_up),
+        (place, mixture_input, mixture_gain[None], routes.T, shared_gate.T, shared_up.T),
         smem=1,
+        limit=12,
     )
     query = call(
         query_kernel,
-        shape((PLAIN + 6 * ROTARY, tokens)),
+        shape((tokens, PLAIN + 6 * ROTARY)),
         (
             place,
             compressed_query,
             query_norm_scale[None],
-            query_plain_weight,
-            query_rotary_weight,
+            query_plain_weight.T,
+            query_rotary_weight.T,
             cos,
             sin,
         ),
@@ -298,6 +301,7 @@
         expert_kernel,
         shape((cores, wide, rows, width)),
         (arrived.reshape(cores, wide, rows, width), expert_gate[0], expert_up[0], down),
+        limit=16,
     )
     parts = exchange(partial.reshape(cores * wide, rows, width), PLANE)
     summed = call(
@@ -307,14 +311,14 @@
     )
     returned = exchange(summed.reshape(planes, cores * capacity, width), "z")
 
-    both = pl.pallas_call(
-        attention_kernel,
-        out_shape=shape((wide, VALUE + shared_units, tokens)),
-        in_specs=[VMEM] * 5,
-        out_specs=VMEM,
-        scratch_shapes=[pltpu.VMEM((tokens, tokens * experts), F32)],
-        cost_estimate=pl.CostEstimate(flops=10**9, bytes_accessed=10**6, transcendentals=0),
-    )(query, all_kv, shared, cos, sin)
+    both = call(
+        functools.partial(attention_kernel, order=behind),
+        shape((wide, VALUE + shared_units, tokens)),
+        (place, query, mine, other, shared, cos, sin),
+        smem=1,
+        scratch=[pltpu.VMEM((tokens, tokens * experts), F32)],
+        limit=12,
+    )
     both = exchange(both, TP)
     return call(
         final_kernel,
@@ -322,7 +326,7 @@
         (
             returned.reshape(experts * capacity, width),
             slots,
-            route_weight,
+            route_weight.T,
             both,
             output_weight,
             shared_down,
@@ -354,6 +358,7 @@
         P(None, TP),
         P(None, TP),
     )
+
     return jax.shard_map(
         per_device,
         mesh=split,

time: 196 us -> 166 us (0.85)
  waiting for transfers between devices: 82.1 us -> 53.3 us
  blocking collectives: 28.3 us -> 47.4 us
  Pallas kernels: 25.6 us -> 12.1 us
  between operations: 14.1 us -> 1.02 us
  starting transfers between devices: 30.5 us -> 42.9 us
  local copies, waits for them, and re-layouts: 13.5 us -> 8.02 us
    all_gather x1 -> x0, waiting for transfers between devices: 30.8 us -> none  [per_device(): lax.all_gather(kv, EP, axis=0, tiled=True).reshape(experts, *kv.shape)]
    ppermute x0 -> x5, waiting for transfers between devices: none -> 26.1 us  [the longest x4 25.3 us: per_device(): received = lax.ppermute(mine, 'z', ring)]
    all_to_all x5 -> x4, waiting for transfers between devices: 51.4 us -> 27.2 us  [exchange(): return lax.all_to_all(array, axes, 0, 0, tiled=True)]
    ppermute x0 -> x5, starting transfers between devices: none -> 20.7 us  [the longest x4 18.8 us: per_device(): received = lax.ppermute(mine, 'z', ring)]
    all_to_all x1 -> x2, blocking collectives: 28.3 us -> 47.4 us  [exchange(): return lax.all_to_all(array, axes, 0, 0, tiled=True)]
    pallas_call x7 -> x8, Pallas kernels: 20.6 us -> 12.1 us  [call(): pl.pallas_call(body, out_shape=outs, in_specs=[SMEM] * smem + [VMEM] * (l...]
    all_to_all x5 -> x4, starting transfers between devices: 30.5 us -> 22.1 us  [exchange(): return lax.all_to_all(array, axes, 0, 0, tiled=True)]
    pallas_call x1 -> x0, Pallas kernels: 4.99 us -> none  [per_device(): pl.pallas_call(attention_kernel, out_shape=shape((wide, VALUE + shared_un...]
  transfers between devices with their start and end apart: 6 -> 9, of which waited for: 5 -> 7; matrix products, arithmetic and copies ran while one was open for 3% -> 1% of each run, Pallas kernels for 10% -> 6%
where the time goes in v2:
time: 166 us; the launch traced here: 165 us
  waiting for transfers between devices  53.3 us (32%)
  blocking collectives  47.4 us (29%)
  starting transfers between devices  42.9 us (26%)
  Pallas kernels  12.1 us (7%)
  local copies, waits for them, and re-layouts  8.02 us (5%)
    all_to_all x2, blocking collectives, exchange(): return lax.all_to_all(array, axes, 0, 0, tiled=True)  47.4 us
    all_to_all x4, waiting for transfers between devices, exchange(): return lax.all_to_all(array, axes, 0, 0, tiled=True)  27.2 us
    ppermute x4, waiting for transfers between devices, per_device(): received = lax.ppermute(mine, 'z', ring)  25.3 us
    all_to_all x4, starting transfers between devices, exchange(): return lax.all_to_all(array, axes, 0, 0, tiled=True)  22.1 us
    ppermute x4, starting transfers between devices, per_device(): received = lax.ppermute(mine, 'z', ring)  18.8 us
    pallas_call x8, Pallas kernels, call(): pl.pallas_call(body, out_shape=outs, in_specs=[SMEM] * smem + [VMEM] * (l...  12.1 us
    unnamed x50, local copies, waits for them, and re-layouts  7.97 us
  transfers between devices with their start and end apart: 9, of which 7 were waited for; matrix products, arithmetic and copies ran while one was open for 1% of the time, Pallas kernels for 6%

profile of v2, /device:TPU:32, one launch (start us, length us, event | category | flops | bytes accessed | tf_op | source)
XLA Modules:
  0.0 165.4 jit_solution(4927306561420121990)
XLA Ops:
  0.7 1.0 copy-done.3
  1.8 0.9 copy-done.7
  2.7 0.9 copy-done.8
  3.6 0.7 copy-done.14
  4.3 0.7 copy-done.17
  4.9 1.7 %shard_map.230 = (bf16[384,128]{1,0:T(8,128)(2,1)S(1)}, s32[2,128]{1,0:T(2,128)S(1)}, bf16[32,128]{1,0:T(8,128)(2,1)S(1)}, bf16[128,2048]{1,0:T(8,128)(2,1)}) custom-call(s32[4]{0:T(128)S(1)} %pad_add_fusion.place, bf16[128,2048]{1,0:T(8,128)(2,1)S(1)} %copy-done.3, f32[1,2048]{1,0:T(1,128)S(1)} %bitcast.47, s32[2,128]{1,0:T(2,128)S(1)} %bitcast.50, ...), custom_call_target="tpu_custom_call" | custom-call | flops 1000000000 | bytes 1000000 | tf_op jit(solution)/shard_map/pallas_call | solution.py:29
  6.7 28.1 %all_to_all.30 = bf16[16,24,128]{2,1,0:T(8,128)(2,1)S(1)} all-to-all(bf16[16,24,128]{2,1,0:T(8,128)(2,1)S(1)} %bitcast.40), channel_id=1, replica_groups=mesh['z'=16,'core'=2,'y'=4,'x'=4] {'z'}, dimensions={0} | all-to-all | bytes 196608 | tf_op jit(solution)/shard_map/all_to_all | solution.py:204
  34.8 7.0 %all-to-all-start.2 = ((bf16[16,256,128]{2,1,0:T(8,128)(2,1)}), bf16[16,256,128]{2,1,0:T(8,128)(2,1)S(1)}, u32[]{:S(2)}, u32[]{:S(2)}) async-start(bf16[16,256,128]{2,1,0:T(8,128)(2,1)} %bitcast.14), calls=%async_computation.2 | async-start | bytes 2097152 | tf_op jit(solution)/shard_map/all_to_all | solution.py:204
  42.2 1.2 copy-done
  43.4 13.9 %all-to-all-done.2.down = bf16[16,256,128]{2,1,0:T(8,128)(2,1)S(1)} async-done(((bf16[16,256,128]{2,1,0:T(8,128)(2,1)}), bf16[16,256,128]{2,1,0:T(8,128)(2,1)S(1)}, u32[]{:S(2)}, u32[]{:S(2)}) %all-to-all-start.2) | async-done | bytes 1048608 | tf_op jit(solution)/shard_map/all_to_all | solution.py:204
  57.3 4.1 %all-to-all-start.1 = ((bf16[32,192,128]{2,1,0:T(8,128)(2,1)}), bf16[32,192,128]{2,1,0:T(8,128)(2,1)S(1)}, u32[]{:S(2)}, u32[]{:S(2)}) async-start(bf16[32,192,128]{2,1,0:T(8,128)(2,1)} %bitcast.30), calls=%async_computation.1 | async-start | bytes 3145728 | tf_op jit(solution)/shard_map/all_to_all | solution.py:204
  61.8 5.0 %collective-permute-start = (bf16[1,160,128]{2,1,0:T(8,128)(2,1)S(1)}, bf16[1,160,128]{2,1,0:T(8,128)(2,1)S(1)}, u32[]{:S(2)}, u32[]{:S(2)}) collective-permute-start(bf16[1,160,128]{2,1,0:T(8,128)(2,1)S(1)} %bitcast.33), channel_id=1, source_target_pairs={{0,256},{32,288},{64,320},{96,352},{128,384},{160,416},{192,448},{... | collective-permute-start | bytes 122888 | tf_op jit(solution)/shard_map/ppermute | solution.py:259
  66.8 9.6 %collective-permute-done = bf16[1,160,128]{2,1,0:T(8,128)(2,1)S(1)} collective-permute-done((bf16[1,160,128]{2,1,0:T(8,128)(2,1)S(1)}, bf16[1,160,128]{2,1,0:T(8,128)(2,1)S(1)}, u32[]{:S(2)}, u32[]{:S(2)}) %collective-permute-start) | collective-permute-done | bytes 40992 | tf_op jit(solution)/shard_map/ppermute | solution.py:259
  76.4 5.8 %collective-permute-start.1 = (bf16[2,160,128]{2,1,0:T(8,128)(2,1)S(1)}, bf16[2,160,128]{2,1,0:T(8,128)(2,1)S(1)}, u32[]{:S(2)}, u32[]{:S(2)}) collective-permute-start(bf16[2,160,128]{2,1,0:T(8,128)(2,1)S(1)} %pad_maximum_fusion.2), channel_id=1, source_target_pairs={{0,128},{32,160},{64,192},{96,224},{128,256},{160,288},{192,320},{... | collective-permute-start | bytes 245768 | tf_op jit(solution)/shard_map/ppermute | solution.py:259
  82.2 5.9 %collective-permute-done.1 = bf16[2,160,128]{2,1,0:T(8,128)(2,1)S(1)} collective-permute-done((bf16[2,160,128]{2,1,0:T(8,128)(2,1)S(1)}, bf16[2,160,128]{2,1,0:T(8,128)(2,1)S(1)}, u32[]{:S(2)}, u32[]{:S(2)}) %collective-permute-start.1) | collective-permute-done | bytes 81952 | tf_op jit(solution)/shard_map/ppermute | solution.py:259
  88.1 0.7 pad_maximum_fusion.1
  88.8 5.9 %collective-permute-start.2 = (bf16[4,160,128]{2,1,0:T(8,128)(2,1)}, bf16[4,160,128]{2,1,0:T(8,128)(2,1)S(1)}, u32[]{:S(2)}, u32[]{:S(2)}) collective-permute-start(bf16[4,160,128]{2,1,0:T(8,128)(2,1)} %pad_maximum_fusion.1), channel_id=1, source_target_pairs={{0,64},{32,96},{64,128},{96,160},{128,192},{160,224},{192,256},{22... | collective-permute-start | bytes 491528 | tf_op jit(solution)/shard_map/ppermute | solution.py:259
  94.8 1.2 copy-done.1
  96.0 1.2 copy-done.2
  97.2 3.2 %shard_map.232 = bf16[2,16,192,128]{3,2,1,0:T(8,128)(2,1)} custom-call(bf16[2,16,192,128]{3,2,1,0:T(8,128)(2,1)S(1)} %bitcast.28, bf16[2048,256]{1,0:T(8,128)(2,1)S(1)} %bitcast.31, bf16[2048,256]{1,0:T(8,128)(2,1)S(1)} %bitcast.32, bf16[16,256,128]{2,1,0:T(8,128)(2,1)S(1)} %all-to-all-done.2.down), custom_call_target="tpu_custom_call" | custom-call | flops 1000000000 | bytes 1000000 | tf_op jit(solution)/shard_map/pallas_call | solution.py:29
  100.4 7.3 %all-to-all-start.3 = ((bf16[32,192,128]{2,1,0:T(8,128)(2,1)}), bf16[32,192,128]{2,1,0:T(8,128)(2,1)S(1)}, u32[]{:S(2)}, u32[]{:S(2)}) async-start(bf16[32,192,128]{2,1,0:T(8,128)(2,1)} %bitcast.15), calls=%async_computation.3 | async-start | bytes 3145728 | tf_op jit(solution)/shard_map/all_to_all | solution.py:204
  107.9 2.1 %collective-permute-start.3 = (bf16[8,160,128]{2,1,0:T(8,128)(2,1)S(1)}, bf16[8,160,128]{2,1,0:T(8,128)(2,1)S(1)}, u32[]{:S(2)}, u32[]{:S(2)}) collective-permute-start(bf16[8,160,128]{2,1,0:T(8,128)(2,1)S(1)} %pad_maximum_fusion), channel_id=1, source_target_pairs={{0,32},{32,64},{64,96},{96,128},{128,160},{160,192},{192,224},{224... | collective-permute-start | bytes 983048 | tf_op jit(solution)/shard_map/ppermute | solution.py:259
  110.0 9.8 %collective-permute-done.3 = bf16[8,160,128]{2,1,0:T(8,128)(2,1)S(1)} collective-permute-done((bf16[8,160,128]{2,1,0:T(8,128)(2,1)S(1)}, bf16[8,160,128]{2,1,0:T(8,128)(2,1)S(1)}, u32[]{:S(2)}, u32[]{:S(2)}) %collective-permute-start.3) | collective-permute-done | bytes 327712 | tf_op jit(solution)/shard_map/ppermute | solution.py:259
  119.9 1.9 %collective-permute-start.4 = (bf16[16,160,128]{2,1,0:T(8,128)(2,1)S(1)}, bf16[16,160,128]{2,1,0:T(8,128)(2,1)S(1)}, u32[]{:S(2)}, u32[]{:S(2)}) collective-permute-start(bf16[16,160,128]{2,1,0:T(8,128)(2,1)S(1)} %constant_dynamic-update-slice_fusion.mine), channel_id=1, source_target_pairs={{0,16},{16,0},{1,17},{17,1},{2,18},{18,2},{3,19},{19,3},{4,20},{20... | collective-permute-start | bytes 1966088 | tf_op jit(solution)/shard_map/ppermute | solution.py:263
  121.9 1.1 shard_map.234.query
  123.0 0.8 collective-permute-done.4.other
  123.9 4.0 %shard_map.236 = bf16[16,96,128]{2,1,0:T(8,128)(2,1)} custom-call(s32[4]{0:T(128)S(1)} %pad_add_fusion.place, bf16[128,256]{1,0:T(8,128)(2,1)S(1)} %shard_map.234.query, bf16[16,160,128]{2,1,0:T(8,128)(2,1)S(1)} %constant_dynamic-update-slice_fusion.mine, bf16[16,160,128]{2,1,0:T(8,128)(2,1)S(1)} %collective-permute-done.4.other, ...), custom_call_target="tpu_custom_call" | custom-call | flops 1000000000 | bytes 1000000 | tf_op jit(solution)/shard_map/pallas_call | solution.py:29
  127.8 3.3 %all-to-all-done.3 = bf16[32,192,128]{2,1,0:T(8,128)(2,1)S(1)} async-done(((bf16[32,192,128]{2,1,0:T(8,128)(2,1)}), bf16[32,192,128]{2,1,0:T(8,128)(2,1)S(1)}, u32[]{:S(2)}, u32[]{:S(2)}) %all-to-all-start.3) | async-done | bytes 1572896 | tf_op jit(solution)/shard_map/all_to_all | solution.py:204
  131.1 3.7 %all-to-all-start.5 = ((bf16[16,96,128]{2,1,0:T(8,128)(2,1)}), bf16[16,96,128]{2,1,0:T(8,128)(2,1)S(1)}, u32[]{:S(2)}, u32[]{:S(2)}) async-start(bf16[16,96,128]{2,1,0:T(8,128)(2,1)} %shard_map.236), calls=%async_computation.5 | async-start | bytes 786432 | tf_op jit(solution)/shard_map/all_to_all | solution.py:204
  135.3 9.9 %all-to-all-done.5.both = bf16[16,96,128]{2,1,0:T(8,128)(2,1)S(1)} async-done(((bf16[16,96,128]{2,1,0:T(8,128)(2,1)}), bf16[16,96,128]{2,1,0:T(8,128)(2,1)S(1)}, u32[]{:S(2)}, u32[]{:S(2)}) %all-to-all-start.5) | async-done | bytes 393248 | tf_op jit(solution)/shard_map/all_to_all | solution.py:204
  145.2 19.2 %all_to_all.31 = bf16[16,24,128]{2,1,0:T(8,128)(2,1)S(1)} all-to-all(bf16[16,24,128]{2,1,0:T(8,128)(2,1)S(1)} %bitcast.37), channel_id=1, replica_groups=mesh['z'=16,'core'=2,'y'=4,'x'=4] {'z'}, dimensions={0} | all-to-all | bytes 196608 | tf_op jit(solution)/shard_map/all_to_all | solution.py:204
  164.5 1.0 shard_map.237
  (52 shorter events, 1.4 us)
Async XLA Ops:
  0.7 1.0 copy-start.3
  1.8 0.9 copy-start.7
  2.7 0.9 copy-start.8
  3.6 0.7 copy-start.14
  4.3 0.7 copy-start.17
  6.7 35.2 %copy-start.19 = (bf16[384,384]{1,0:T(8,128)(2,1)S(1)}, bf16[384,384]{1,0:T(8,128)(2,1)}, u32[]{:S(2)}) copy-start(bf16[384,384]{1,0:T(8,128)(2,1)} %constant.28.clone.order) | copy-start | bytes 884740
  34.8 22.5 %all-to-all-start.2 = ((bf16[16,256,128]{2,1,0:T(8,128)(2,1)}), bf16[16,256,128]{2,1,0:T(8,128)(2,1)S(1)}, u32[]{:S(2)}, u32[]{:S(2)}) async-start(bf16[16,256,128]{2,1,0:T(8,128)(2,1)} %bitcast.14), calls=%async_computation.2 | async-start | bytes 2097152 | tf_op jit(solution)/shard_map/all_to_all | solution.py:204
  42.2 1.2 copy-start
  57.3 4.1 %copy-start.9 = (bf16[128,512]{1,0:T(8,128)(2,1)S(1)}, bf16[128,512]{1,0:T(8,128)(2,1)}, u32[]{:S(2)}) copy-start(bf16[128,512]{1,0:T(8,128)(2,1)} %latent.3) | copy-start | bytes 393220
  57.3 4.2 %copy-start.12 = (bf16[512,64]{0,1:T(8,128)(2,1)S(1)}, bf16[512,64]{0,1:T(8,128)(2,1)}, u32[]{:S(2)}) copy-start(bf16[512,64]{0,1:T(8,128)(2,1)} %param.30) | copy-start | bytes 196612
  57.3 4.2 %copy-start.13 = (bf16[512,64]{0,1:T(8,128)(2,1)S(1)}, bf16[512,64]{0,1:T(8,128)(2,1)}, u32[]{:S(2)}) copy-start(bf16[512,64]{0,1:T(8,128)(2,1)} %param.31) | copy-start | bytes 196612
  57.3 4.2 %copy-start.15 = (bf16[128,32]{0,1:T(8,128)(2,1)S(1)}, bf16[128,32]{0,1:T(8,128)(2,1)}, u32[]{:S(2)}) copy-start(bf16[128,32]{0,1:T(8,128)(2,1)} %param.25) | copy-start | bytes 24580
  57.3 4.2 %copy-start.16 = (f32[512]{0:T(512)S(1)}, f32[512]{0:T(512)}, u32[]{:S(2)}) copy-start(f32[512]{0:T(512)} %param.27) | copy-start | bytes 6148
  57.3 37.5 %all-to-all-start.1 = ((bf16[32,192,128]{2,1,0:T(8,128)(2,1)}), bf16[32,192,128]{2,1,0:T(8,128)(2,1)S(1)}, u32[]{:S(2)}, u32[]{:S(2)}) async-start(bf16[32,192,128]{2,1,0:T(8,128)(2,1)} %bitcast.30), calls=%async_computation.1 | async-start | bytes 3145728 | tf_op jit(solution)/shard_map/all_to_all | solution.py:204
  61.8 14.6 %collective-permute-start = (bf16[1,160,128]{2,1,0:T(8,128)(2,1)S(1)}, bf16[1,160,128]{2,1,0:T(8,128)(2,1)S(1)}, u32[]{:S(2)}, u32[]{:S(2)}) collective-permute-start(bf16[1,160,128]{2,1,0:T(8,128)(2,1)S(1)} %bitcast.33), channel_id=1, source_target_pairs={{0,256},{32,288},{64,320},{96,352},{128,384},{160,416},{192,448},{... | collective-permute-start | bytes 122888 | tf_op jit(solution)/shard_map/ppermute | solution.py:259
  76.4 11.7 %collective-permute-start.1 = (bf16[2,160,128]{2,1,0:T(8,128)(2,1)S(1)}, bf16[2,160,128]{2,1,0:T(8,128)(2,1)S(1)}, u32[]{:S(2)}, u32[]{:S(2)}) collective-permute-start(bf16[2,160,128]{2,1,0:T(8,128)(2,1)S(1)} %pad_maximum_fusion.2), channel_id=1, source_target_pairs={{0,128},{32,160},{64,192},{96,224},{128,256},{160,288},{192,320},{... | collective-permute-start | bytes 245768 | tf_op jit(solution)/shard_map/ppermute | solution.py:259
  88.8 19.0 %collective-permute-start.2 = (bf16[4,160,128]{2,1,0:T(8,128)(2,1)}, bf16[4,160,128]{2,1,0:T(8,128)(2,1)S(1)}, u32[]{:S(2)}, u32[]{:S(2)}) collective-permute-start(bf16[4,160,128]{2,1,0:T(8,128)(2,1)} %pad_maximum_fusion.1), channel_id=1, source_target_pairs={{0,64},{32,96},{64,128},{96,160},{128,192},{160,224},{192,256},{22... | collective-permute-start | bytes 491528 | tf_op jit(solution)/shard_map/ppermute | solution.py:259
  94.8 1.2 copy-start.1
  96.0 1.2 copy-start.2
  100.4 30.7 %all-to-all-start.3 = ((bf16[32,192,128]{2,1,0:T(8,128)(2,1)}), bf16[32,192,128]{2,1,0:T(8,128)(2,1)S(1)}, u32[]{:S(2)}, u32[]{:S(2)}) async-start(bf16[32,192,128]{2,1,0:T(8,128)(2,1)} %bitcast.15), calls=%async_computation.3 | async-start | bytes 3145728 | tf_op jit(solution)/shard_map/all_to_all | solution.py:204
  107.7 14.0 %copy-start.22 = (f32[1536]{0:T(1024)S(1)}, f32[1536]{0:T(1024)}, u32[]{:S(2)}) copy-start(f32[1536]{0:T(1024)} %param.26) | copy-start | bytes 18436
  107.8 14.1 %copy-start.4 = (bf16[128,1536]{1,0:T(8,128)(2,1)S(1)}, bf16[128,1536]{1,0:T(8,128)(2,1)}, u32[]{:S(2)}) copy-start(bf16[128,1536]{1,0:T(8,128)(2,1)} %latent.2) | copy-start | bytes 1179652
  107.8 14.1 %copy-start.6 = (bf16[1536,64]{0,1:T(8,128)(2,1)S(1)}, bf16[1536,64]{0,1:T(8,128)(2,1)}, u32[]{:S(2)}) copy-start(bf16[1536,64]{0,1:T(8,128)(2,1)} %param.28) | copy-start | bytes 589828
  107.8 14.0 %copy-start.11 = (bf16[1536,32]{0,1:T(8,128)(2,1)S(1)}, bf16[1536,32]{0,1:T(8,128)(2,1)}, u32[]{:S(2)}) copy-start(bf16[1536,32]{0,1:T(8,128)(2,1)} %param.29) | copy-start | bytes 294916
  107.8 14.0 %copy-start.20 = (f32[32,16,128]{2,1,0:T(8,128)S(1)}, f32[32,16,128]{2,1,0:T(8,128)}, u32[]{:S(2)}) copy-start(f32[32,16,128]{2,1,0:T(8,128)} %constant.29.clone.cos) | copy-start | bytes 786436
  107.8 14.0 %copy-start.21 = (f32[32,16,128]{2,1,0:T(8,128)S(1)}, f32[32,16,128]{2,1,0:T(8,128)}, u32[]{:S(2)}) copy-start(f32[32,16,128]{2,1,0:T(8,128)} %constant.30.clone.sin) | copy-start | bytes 786436
  107.9 11.9 %collective-permute-start.3 = (bf16[8,160,128]{2,1,0:T(8,128)(2,1)S(1)}, bf16[8,160,128]{2,1,0:T(8,128)(2,1)S(1)}, u32[]{:S(2)}, u32[]{:S(2)}) collective-permute-start(bf16[8,160,128]{2,1,0:T(8,128)(2,1)S(1)} %pad_maximum_fusion), channel_id=1, source_target_pairs={{0,32},{32,64},{64,96},{96,128},{128,160},{160,192},{192,224},{224... | collective-permute-start | bytes 983048 | tf_op jit(solution)/shard_map/ppermute | solution.py:259
  119.9 4.0 %collective-permute-start.4 = (bf16[16,160,128]{2,1,0:T(8,128)(2,1)S(1)}, bf16[16,160,128]{2,1,0:T(8,128)(2,1)S(1)}, u32[]{:S(2)}, u32[]{:S(2)}) collective-permute-start(bf16[16,160,128]{2,1,0:T(8,128)(2,1)S(1)} %constant_dynamic-update-slice_fusion.mine), channel_id=1, source_target_pairs={{0,16},{16,0},{1,17},{17,1},{2,18},{18,2},{3,19},{19,3},{4,20},{20... | collective-permute-start | bytes 1966088 | tf_op jit(solution)/shard_map/ppermute | solution.py:263
  131.1 14.1 %all-to-all-start.5 = ((bf16[16,96,128]{2,1,0:T(8,128)(2,1)}), bf16[16,96,128]{2,1,0:T(8,128)(2,1)S(1)}, u32[]{:S(2)}, u32[]{:S(2)}) async-start(bf16[16,96,128]{2,1,0:T(8,128)(2,1)} %shard_map.236), calls=%async_computation.5 | async-start | bytes 786432 | tf_op jit(solution)/shard_map/all_to_all | solution.py:204
  134.8 29.6 %copy-start.5 = (bf16[1024,128]{1,0:T(8,128)(2,1)S(1)}, bf16[1024,128]{1,0:T(8,128)(2,1)}, u32[]{:S(2)}) copy-start(bf16[1024,128]{1,0:T(8,128)(2,1)} %output_weight.1) | copy-start | bytes 786436
  134.8 29.6 %copy-start.10 = (bf16[512,128]{1,0:T(8,128)(2,1)S(1)}, bf16[512,128]{1,0:T(8,128)(2,1)}, u32[]{:S(2)}) copy-start(bf16[512,128]{1,0:T(8,128)(2,1)} %shared_down.1) | copy-start | bytes 393220
  134.8 29.6 %copy-start.18 = (f32[128,2]{0,1:T(2,128)S(1)}, f32[128,2]{0,1:T(2,128)}, u32[]{:S(2)}) copy-start(f32[128,2]{0,1:T(2,128)} %param.36) | copy-start | bytes 3076

commit v3 on v2

--- a/solution.py
+++ b/solution.py
@@ -14,7 +14,6 @@
 VALUE = 64
 EP = ("z", "core")
 TP = ("y", "x")
-PLANE = ("core", "y", "x")
 F32 = jnp.float32
 BF16 = jnp.bfloat16
 VMEM = pl.BlockSpec(memory_space=pltpu.VMEM)
@@ -74,40 +73,35 @@
     out[...] = whole.astype(F32).T.astype(BF16)
 
 
-def attention_kernel(place, query, mine, other, shared, cos, sin, out, scores, *, order):
+def attention_kernel(query, kv, shared, cos, sin, out, scores):
     q = query[...]
-    planes, _, width = mine.shape
+    blocks, _, width = kv.shape
     half = ROTARY // 2
     scale = (PLAIN + ROTARY) ** -0.5
     tokens = q.shape[0]
-    blocks = [(kv, j) for kv in (mine, other) for j in range(planes)]
 
     top = jnp.full((tokens, width), -jnp.inf, F32)
-    for n, (kv, j) in enumerate(blocks):
-        core = place[2] if kv is mine else 1 - place[2]
-        at = ((place[1] + (planes - order[j])) % planes) * 2 + core
+    for j in range(blocks):
         raw = kv[j, PLAIN + VALUE :, :].astype(F32)
         a, b = raw[0:half, :], raw[half:, :]
-        c, s = cos[at], sin[at]
+        c, s = cos[j], sin[j]
         high, middle, low = split3(jnp.concatenate([a * c - b * s, a * s + b * c], axis=0))
         keys = jnp.concatenate(
             [kv[j, 0:PLAIN, :], high, middle, high, middle, low, high], axis=0
         )
         part = dot(q, keys) * scale
-        scores[:, n * width : (n + 1) * width] = part
+        scores[:, j * width : (j + 1) * width] = part
         top = jnp.maximum(top, part)
     largest = jnp.max(top, axis=1, keepdims=True)
     total = jnp.zeros((tokens, width), F32)
     summed = jnp.zeros((VALUE, tokens), F32)
-    for n, (kv, j) in enumerate(blocks):
-        weights = jnp.exp(scores[:, n * width : (n + 1) * width] - largest)
+    for j in range(blocks):
+        weights = jnp.exp(scores[:, j * width : (j + 1) * width] - largest)
         total = total + weights
         summed = summed + dot(kv[j, PLAIN : PLAIN + VALUE, :], weights.astype(BF16), 1, 1)
     whole = jnp.broadcast_to(jnp.sum(total, axis=1, keepdims=True), (tokens, width)).T
     heads = (summed / whole[0:VALUE, :]).astype(BF16)
-    sent = jnp.concatenate([heads, shared[...]], axis=0)
-    for t in range(out.shape[0]):
-        out[t] = sent
+    out[0] = jnp.concatenate([heads, shared[...]], axis=0)
 
 
 def one_hot(slots, k, rows):
@@ -142,24 +136,36 @@
     shared[...] = (g / (1.0 + jnp.exp(-g)) * u).astype(BF16)
 
 
-def spread_kernel(order, rows, out):
-    placed = dot(order[...], rows[...]).astype(BF16)
-    half = out.shape[2]
-    for c in range(out.shape[0]):
-        part = placed[c * half : (c + 1) * half, :]
-        for t in range(out.shape[1]):
-            out[c, t] = part
-
-
-def expert_kernel(rows, gate, up, down, out):
-    parts, wide = rows.shape[0], rows.shape[1]
+def order_kernel(order, rows, out):
+    out[...] = dot(order[...], rows[...]).astype(BF16)
+
+
+def spread_kernel(rows, out):
+    for t in range(out.shape[0]):
+        out[t] = rows[...]
+
+
+def hidden_kernel(rows, gate, up, out, *, parts):
+    wide, length = rows.shape[0], rows.shape[1] // parts
     for c in range(parts):
-        x = jnp.concatenate([rows[c, t] for t in range(wide)], axis=1)
+        part = slice(c * length, (c + 1) * length)
+        x = jnp.concatenate([rows[t, part, :] for t in range(wide)], axis=1)
         g = dot(x, gate[...])
         u = dot(x, up[...])
         hidden = (g / (1.0 + jnp.exp(-g)) * u).astype(BF16)
-        for t in range(wide):
-            out[c, t] = dot(hidden, down[t]).astype(BF16)
+        for t in range(out.shape[0]):
+            out[t, part, :] = hidden
+
+
+def down_kernel(place, hidden, *rest):
+    downs, out = rest[:-1], rest[-1]
+    parts, tall, length = out.shape[0], out.shape[1], out.shape[2]
+    x = jnp.concatenate([hidden[t] for t in range(hidden.shape[0])], axis=1)
+    for k, down in enumerate(downs):
+        to = (place[4] + (tall - k)) % tall
+        result = dot(x, down[...]).astype(BF16)
+        for c in range(parts):
+            out[c, to] = result[c * length : (c + 1) * length, :]
 
 
 def gathered_sum_kernel(order, partial, out):
@@ -173,17 +179,27 @@
     out[...] = dot(order[...], jnp.concatenate(sums, axis=0), 0, 0).astype(BF16)
 
 
-def final_kernel(returned, slots, route_weight, both, output_weight, shared_down, attended, combined):
+def final_kernel(place, returned, slots, route_weight, output_weight, shared_down, *rest):
+    both, (attended, combined) = rest[:-2], rest[-2:]
     tokens, width = slots.shape[1], returned.shape[1]
     routed = jnp.zeros((tokens, width), F32)
     for k in range(slots.shape[0]):
         hot = one_hot(slots, k, returned.shape[0]).astype(BF16)
         scale = jnp.broadcast_to(route_weight[k : k + 1, :], (width, tokens)).T
         routed = routed + dot(hot, returned[...], 0, 0) * scale
-    heads = jnp.concatenate([both[t, 0:VALUE, :] for t in range(both.shape[0])], axis=0)
-    hidden = jnp.concatenate([both[t, VALUE:, :] for t in range(both.shape[0])], axis=0)
-    attended[...] = dot(heads, output_weight[...], 0, 0).astype(BF16)
-    combined[...] = (dot(hidden, shared_down[...], 0, 0) + routed).astype(BF16)
+    tall, across = len(both), both[0].shape[0]
+    units = both[0].shape[1] - VALUE
+    heads, hidden, heads_weight, hidden_weight = [], [], [], []
+    for a in range(tall):
+        for b in range(across):
+            at = (place[4] + (tall - a)) % tall * across + (place[5] + (across - b)) % across
+            heads.append(both[a][b, 0:VALUE, :])
+            hidden.append(both[a][b, VALUE:, :])
+            heads_weight.append(output_weight[pl.ds(pl.multiple_of(at * VALUE, VALUE), VALUE), :])
+            hidden_weight.append(shared_down[pl.ds(pl.multiple_of(at * units, units), units), :])
+    joined = [jnp.concatenate(p, axis=0) for p in (heads, heads_weight, hidden, hidden_weight)]
+    attended[...] = dot(joined[0], joined[1], 0, 0).astype(BF16)
+    combined[...] = (dot(joined[2], joined[3], 0, 0) + routed).astype(BF16)
 
 
 def tables(positions, width):
@@ -234,13 +250,20 @@
     capacity = tokens * routes.shape[1] * 3 // (2 * experts)
     units = expert_gate.shape[2]
     shared_units = shared_gate.shape[1]
+    tall, across = lax.axis_size("y"), lax.axis_size("x")
+    row = lax.axis_index("y")
     place = jnp.stack(
-        [lax.axis_index(EP), lax.axis_index("z"), lax.axis_index("core"), lax.axis_index(TP)]
+        [
+            lax.axis_index(EP),
+            lax.axis_index("z"),
+            lax.axis_index("core"),
+            lax.axis_index(TP),
+            row,
+            lax.axis_index("x"),
+        ]
     ).astype(jnp.int32)
     cos, sin = tables(tokens * experts, tokens)
     order = jnp.asarray(row_order(planes, cores, capacity), BF16)
-
-    down = exchange(expert_down[0].reshape(wide, units, width), TP)
 
     kv = call(
         key_value_kernel,
@@ -252,15 +275,17 @@
             value_up_weight.T,
             rotary_key.T,
         ),
-    )
-    mine, behind, step = kv[None], [0], planes // 2
-    while step:
-        ring = [(z, (z + step) % planes) for z in range(planes)]
-        received = lax.ppermute(mine, "z", ring)
-        mine = jnp.concatenate([mine, received], axis=0)
-        behind = behind + [(b + step) % planes for b in behind]
-        step //= 2
-    other = lax.ppermute(mine, "core", [(0, 1), (1, 0)])
+        limit=56,
+    )
+    all_kv = lax.all_gather(kv, EP, axis=0, tiled=True).reshape(experts, *kv.shape)
+
+    band = across * units
+    downs = []
+    for k in range(tall):
+        part = lax.dynamic_slice_in_dim(expert_down[0], (row + k) % tall * band, band, 0)
+        if k:
+            part = lax.ppermute(part, "y", [(y, (y + k) % tall) for y in range(tall)])
+        downs.append(part)
 
     sent, slots, shared, _ = call(
         functools.partial(dispatch_kernel, experts=experts, capacity=capacity),
@@ -291,46 +316,67 @@
 
     moved = exchange(sent.reshape(planes, cores * capacity, width), "z")
     rows = planes * capacity
+    moved = call(
+        order_kernel,
+        shape((experts * capacity, width)),
+        (order, moved.reshape(experts * capacity, width)),
+    )
+    moved = exchange(moved.reshape(cores, rows, width), "core")
     spread = call(
         spread_kernel,
-        shape((cores, wide, rows, width)),
-        (order, moved.reshape(experts * capacity, width)),
-    )
-    arrived = exchange(spread.reshape(cores * wide, rows, width), PLANE)
+        shape((wide, cores * rows, width)),
+        (moved.reshape(cores * rows, width),),
+    )
+    arrived = exchange(spread, TP)
+    hidden = call(
+        functools.partial(hidden_kernel, parts=cores),
+        shape((across, cores * rows, units)),
+        (arrived, expert_gate[0], expert_up[0]),
+        limit=14,
+    )
+    hidden = exchange(hidden, "x")
     partial = call(
-        expert_kernel,
-        shape((cores, wide, rows, width)),
-        (arrived.reshape(cores, wide, rows, width), expert_gate[0], expert_up[0], down),
-        limit=16,
-    )
-    parts = exchange(partial.reshape(cores * wide, rows, width), PLANE)
+        down_kernel,
+        shape((cores, tall, rows, width)),
+        (place, hidden, *downs),
+        smem=1,
+        limit=10,
+    )
+    parts = exchange(partial.reshape(cores * tall, rows, width), ("core", "y"))
     summed = call(
         gathered_sum_kernel,
         shape((experts * capacity, width)),
-        (order, parts.reshape(cores, wide, rows, width)),
+        (order, parts.reshape(cores, tall, rows, width)),
     )
     returned = exchange(summed.reshape(planes, cores * capacity, width), "z")
 
     both = call(
-        functools.partial(attention_kernel, order=behind),
-        shape((wide, VALUE + shared_units, tokens)),
-        (place, query, mine, other, shared, cos, sin),
-        smem=1,
+        attention_kernel,
+        shape((1, VALUE + shared_units, tokens)),
+        (query, all_kv, shared, cos, sin),
         scratch=[pltpu.VMEM((tokens, tokens * experts), F32)],
         limit=12,
     )
-    both = exchange(both, TP)
+    pieces = [both]
+    for k in range(1, across):
+        pieces.append(lax.ppermute(both, "x", [(x, (x + k) % across) for x in range(across)]))
+    both = jnp.concatenate(pieces, axis=0)
+    pieces = [both]
+    for k in range(1, tall):
+        pieces.append(lax.ppermute(both, "y", [(y, (y + k) % tall) for y in range(tall)]))
     return call(
         final_kernel,
         (shape((tokens, width)), shape((tokens, width))),
         (
+            place,
             returned.reshape(experts * capacity, width),
             slots,
             route_weight.T,
-            both,
             output_weight,
             shared_down,
+            *pieces,
         ),
+        smem=1,
     )
 
 

time: 166 us -> 167 us (level)
  blocking collectives: 47.4 us -> 31.8 us
  between operations: 1.02 us -> 14.4 us
  starting transfers between devices: 42.9 us -> 47.7 us
  waiting for transfers between devices: 53.3 us -> 49 us
  Pallas kernels: 12.1 us -> 15.8 us
    all_to_all x2, blocking collectives: 47.4 us -> 31.8 us  [exchange(): return lax.all_to_all(array, axes, 0, 0, tiled=True)]
    ppermute x5 -> x9, waiting for transfers between devices: 26.1 us -> 17.6 us  [the longest x3 9.3 us: per_device(): part = lax.ppermute(part, 'y', [(y, (y + k) % tall) for y in range(tall)])]
    ppermute x5 -> x9, starting transfers between devices: 20.7 us -> 28.9 us  [the longest x3 10.3 us: per_device(): lax.ppermute(both, 'x', [(x, (x + k) % across) for x in range(across)])]
    all_to_all x4, waiting for transfers between devices: 27.2 us -> 31.3 us  [exchange(): return lax.all_to_all(array, axes, 0, 0, tiled=True)]
    pallas_call x8 -> x10, Pallas kernels: 12.1 us -> 15.8 us  [call(): pl.pallas_call(body, out_shape=outs, in_specs=[SMEM] * smem + [VMEM] * (l...]
    all_to_all x4, starting transfers between devices: 22.1 us -> 18.7 us  [exchange(): return lax.all_to_all(array, axes, 0, 0, tiled=True)]
    unnamed x50 -> x38, local copies, waits for them, and re-layouts: 7.97 us -> 6.81 us
  transfers between devices with their start and end apart: 9 -> 14, of which waited for: 7 -> 8; matrix products, arithmetic and copies ran while one was open for 1% -> 0% of each run, Pallas kernels for 6% -> 7%
where the time goes in v3:
time: 167 us; the launch traced here: 166 us
  waiting for transfers between devices  49 us (29%)
  starting transfers between devices  47.7 us (29%)
  blocking collectives  31.8 us (19%)
  Pallas kernels  15.8 us (9%)
  between operations  14.4 us (9%)
  local copies, waits for them, and re-layouts  6.98 us (4%)
    all_to_all x2, blocking collectives, exchange(): return lax.all_to_all(array, axes, 0, 0, tiled=True)  31.8 us
    all_to_all x4, waiting for transfers between devices, exchange(): return lax.all_to_all(array, axes, 0, 0, tiled=True)  31.3 us
    all_to_all x4, starting transfers between devices, exchange(): return lax.all_to_all(array, axes, 0, 0, tiled=True)  18.7 us
    pallas_call x10, Pallas kernels, call(): pl.pallas_call(body, out_shape=outs, in_specs=[SMEM] * smem + [VMEM] * (l...  15.8 us
    ppermute x3, starting transfers between devices, per_device(): lax.ppermute(both, 'x', [(x, (x + k) % across) for x in range(across)])  10.3 us
    ppermute x3, starting transfers between devices, per_device(): lax.ppermute(both, 'y', [(y, (y + k) % tall) for y in range(tall)])  9.44 us
    ppermute x3, waiting for transfers between devices, per_device(): part = lax.ppermute(part, 'y', [(y, (y + k) % tall) for y in range(tall)])  9.3 us
    ppermute x3, starting transfers between devices, per_device(): part = lax.ppermute(part, 'y', [(y, (y + k) % tall) for y in range(tall)])  9.2 us
  transfers between devices with their start and end apart: 14, of which 8 were waited for; matrix products, arithmetic and copies ran while one was open for 0% of the time, Pallas kernels for 7%

profile of v3, /device:TPU:32, one launch (start us, length us, event | category | flops | bytes accessed | tf_op | source)
XLA Modules:
  0.0 165.6 jit_solution(2065478029095035058)
XLA Ops:
  11.5 1.7 %shard_map.230 = (bf16[384,128]{1,0:T(8,128)(2,1)S(1)}, s32[2,128]{1,0:T(2,128)S(1)}, bf16[32,128]{1,0:T(8,128)(2,1)S(1)}, bf16[128,2048]{1,0:T(8,128)(2,1)}) custom-call(s32[6]{0:T(128)S(1)} %stack.27.place, bf16[128,2048]{1,0:T(8,128)(2,1)S(1)} %copy-done.3, f32[1,2048]{1,0:T(1,128)S(1)} %bitcast.49, s32[2,128]{1,0:T(2,128)S(1)} %bitcast.50, ...), custom_call_target="tpu_custom_call" | custom-call | flops 1000000000 | bytes 1000000 | tf_op jit(solution)/shard_map/pallas_call | solution.py:28
  13.2 28.0 %all_to_all.30 = bf16[16,24,128]{2,1,0:T(8,128)(2,1)S(1)} all-to-all(bf16[16,24,128]{2,1,0:T(8,128)(2,1)S(1)} %bitcast.40), channel_id=1, replica_groups=mesh['z'=16,'core'=2,'y'=4,'x'=4] {'z'}, dimensions={0} | all-to-all | bytes 196608 | tf_op jit(solution)/shard_map/all_to_all | solution.py:220
  41.5 3.8 %all_to_all.31 = bf16[2,192,128]{2,1,0:T(8,128)(2,1)S(1)} all-to-all(bf16[2,192,128]{2,1,0:T(8,128)(2,1)S(1)} %bitcast.42), channel_id=1, replica_groups=mesh['z'=16,'core'=2,'y'=4,'x'=4] {'core'}, dimensions={0} | all-to-all | bytes 196608 | tf_op jit(solution)/shard_map/all_to_all | solution.py:220
  45.3 1.4 shard_map.232
  46.6 7.0 %all-to-all-start.2 = ((bf16[16,384,128]{2,1,0:T(8,128)(2,1)}), bf16[16,384,128]{2,1,0:T(8,128)(2,1)S(1)}, u32[]{:S(2)}, u32[]{:S(2)}) async-start(bf16[16,384,128]{2,1,0:T(8,128)(2,1)} %shard_map.232), calls=%async_computation.2 | async-start | bytes 3145728 | tf_op jit(solution)/shard_map/all_to_all | solution.py:220
  53.7 2.0 %shard_map.237 = bf16[160,128]{1,0:T(8,128)(2,1)} custom-call(bf16[128,512]{1,0:T(8,128)(2,1)} %latent.3, f32[1,512]{1,0:T(1,128)} %bitcast.55, bf16[64,512]{1,0:T(8,128)(2,1)} %bitcast.52, bf16[64,512]{1,0:T(8,128)(2,1)} %bitcast.53, bf16[32,128]{1,0:T(8,128)(2,1)} %bitcast.54), custom_call_target="tpu_custom_call" | custom-call | flops 1000000000 | bytes 1000000 | tf_op jit(solution)/shard_map/pallas_call | solution.py:28
  55.7 23.1 %all-to-all-done.2.rows = bf16[16,384,128]{2,1,0:T(8,128)(2,1)S(1)} async-done(((bf16[16,384,128]{2,1,0:T(8,128)(2,1)}), bf16[16,384,128]{2,1,0:T(8,128)(2,1)S(1)}, u32[]{:S(2)}, u32[]{:S(2)}) %all-to-all-start.2) | async-done | bytes 1572896 | tf_op jit(solution)/shard_map/all_to_all | solution.py:220
  78.9 1.2 copy-done.1
  80.1 1.9 %shard_map.233 = bf16[4,384,256]{2,1,0:T(8,128)(2,1)} custom-call(bf16[16,384,128]{2,1,0:T(8,128)(2,1)S(1)} %all-to-all-done.2.rows, bf16[2048,256]{1,0:T(8,128)(2,1)S(1)} %bitcast.36, bf16[2048,256]{1,0:T(8,128)(2,1)S(1)} %bitcast.37), custom_call_target="tpu_custom_call" | custom-call | flops 1000000000 | bytes 1000000 | tf_op jit(solution)/shard_map/pallas_call | solution.py:28
  82.0 3.6 %all-to-all-start.3 = ((bf16[4,384,256]{2,1,0:T(8,128)(2,1)}), bf16[4,384,256]{2,1,0:T(8,128)(2,1)S(1)}, u32[]{:S(2)}, u32[]{:S(2)}) async-start(bf16[4,384,256]{2,1,0:T(8,128)(2,1)} %shard_map.233), calls=%async_computation.3 | async-start | bytes 1572864 | tf_op jit(solution)/shard_map/all_to_all | solution.py:220
  85.8 2.2 %collective-permute-start = (bf16[1024,128]{1,0:T(8,128)(2,1)S(1)}, bf16[1024,128]{1,0:T(8,128)(2,1)S(1)}, u32[]{:S(2)}, u32[]{:S(2)}) collective-permute-start(bf16[1024,128]{1,0:T(8,128)(2,1)S(1)} %get-tuple-element.9), channel_id=1, source_target_pairs={{0,4},{4,8},{8,12},{12,0},{1,5},{5,9},{9,13},{13,1},{2,6},{6,10},{... | collective-permute-start | bytes 786440 | tf_op jit(solution)/shard_map/ppermute | solution.py:287
  88.0 4.5 %collective-permute-start.1 = (bf16[1024,128]{1,0:T(8,128)(2,1)S(1)}, bf16[1024,128]{1,0:T(8,128)(2,1)S(1)}, u32[]{:S(2)}, u32[]{:S(2)}) collective-permute-start(bf16[1024,128]{1,0:T(8,128)(2,1)S(1)} %get-tuple-element.11), channel_id=1, source_target_pairs={{0,8},{4,12},{8,0},{12,4},{1,9},{5,13},{9,1},{13,5},{2,10},{6,14},... | collective-permute-start | bytes 786440 | tf_op jit(solution)/shard_map/ppermute | solution.py:287
  92.5 2.5 %collective-permute-start.2 = (bf16[1024,128]{1,0:T(8,128)(2,1)S(1)}, bf16[1024,128]{1,0:T(8,128)(2,1)S(1)}, u32[]{:S(2)}, u32[]{:S(2)}) collective-permute-start(bf16[1024,128]{1,0:T(8,128)(2,1)S(1)} %get-tuple-element.8), channel_id=1, source_target_pairs={{0,12},{4,0},{8,4},{12,8},{1,13},{5,1},{9,5},{13,9},{2,14},{6,2},{... | collective-permute-start | bytes 786440 | tf_op jit(solution)/shard_map/ppermute | solution.py:287
  95.0 6.8 %collective-permute-done.rest_1_ = bf16[1024,128]{1,0:T(8,128)(2,1)S(1)} collective-permute-done((bf16[1024,128]{1,0:T(8,128)(2,1)S(1)}, bf16[1024,128]{1,0:T(8,128)(2,1)S(1)}, u32[]{:S(2)}, u32[]{:S(2)}) %collective-permute-start) | collective-permute-done | bytes 262176 | tf_op jit(solution)/shard_map/ppermute | solution.py:287
  101.8 2.5 %collective-permute-done.2.rest_3_ = bf16[1024,128]{1,0:T(8,128)(2,1)S(1)} collective-permute-done((bf16[1024,128]{1,0:T(8,128)(2,1)S(1)}, bf16[1024,128]{1,0:T(8,128)(2,1)S(1)}, u32[]{:S(2)}, u32[]{:S(2)}) %collective-permute-start.2) | collective-permute-done | bytes 262176 | tf_op jit(solution)/shard_map/ppermute | solution.py:287
  104.3 2.3 %shard_map.234 = bf16[2,4,192,128]{3,2,1,0:T(8,128)(2,1)} custom-call(s32[6]{0:T(128)S(1)} %stack.27.place, bf16[4,384,256]{2,1,0:T(8,128)(2,1)S(1)} %all-to-all-done.3.hidden, bf16[1024,128]{1,0:T(8,128)(2,1)S(1)} %get-tuple-element.10.rest_0_, bf16[1024,128]{1,0:T(8,128)(2,1)S(1)} %collective-permute-done.rest_1_, ...), custom_call_target="tpu_custom_call" | custom-call | flops 1000000000 | bytes 1000000 | tf_op jit(solution)/shard_map/pallas_call | solution.py:28
  106.6 3.9 %all-to-all-start.4 = ((bf16[8,192,128]{2,1,0:T(8,128)(2,1)}), bf16[8,192,128]{2,1,0:T(8,128)(2,1)S(1)}, u32[]{:S(2)}, u32[]{:S(2)}) async-start(bf16[8,192,128]{2,1,0:T(8,128)(2,1)} %bitcast.20), calls=%async_computation.4 | async-start | bytes 786432 | tf_op jit(solution)/shard_map/all_to_all | solution.py:220
  110.5 8.2 %all-to-all-done.4 = bf16[8,192,128]{2,1,0:T(8,128)(2,1)S(1)} async-done(((bf16[8,192,128]{2,1,0:T(8,128)(2,1)}), bf16[8,192,128]{2,1,0:T(8,128)(2,1)S(1)}, u32[]{:S(2)}, u32[]{:S(2)}) %all-to-all-start.4) | async-done | bytes 393248 | tf_op jit(solution)/shard_map/all_to_all | solution.py:220
  119.7 4.2 %all-to-all-start.5 = ((bf16[16,24,128]{2,1,0:T(8,128)(2,1)}), bf16[16,24,128]{2,1,0:T(8,128)(2,1)S(1)}, u32[]{:S(2)}, u32[]{:S(2)}) async-start(bf16[16,24,128]{2,1,0:T(8,128)(2,1)} %bitcast.22), calls=%async_computation.5 | async-start | bytes 196608 | tf_op jit(solution)/shard_map/all_to_all | solution.py:220
  125.1 1.3 copy-done.2
  126.4 2.7 %shard_map.238 = bf16[1,96,128]{2,1,0:T(8,128)(2,1)S(1)} custom-call(bf16[128,256]{1,0:T(8,128)(2,1)S(1)} %shard_map.236.query, bf16[32,160,128]{2,1,0:T(8,128)(2,1)S(1)} %bitcast.44, bf16[32,128]{1,0:T(8,128)(2,1)S(1)} %get-tuple-element.7.shared, f32[32,16,128]{2,1,0:T(8,128)S(1)} %copy-done.15, f32[32,16,128]{2,1,0:T(8,128)S(1)} %copy-done.16), custom_call_target="tpu_custom_call" | custom-call | flops 1000000000 | bytes 1000000 | tf_op jit(solution)/shard_map/pallas_call | solution.py:28
  129.1 4.8 %collective-permute-start.5 = (bf16[1,96,128]{2,1,0:T(8,128)(2,1)S(1)}, bf16[1,96,128]{2,1,0:T(8,128)(2,1)S(1)}, u32[]{:S(2)}, u32[]{:S(2)}) collective-permute-start(bf16[1,96,128]{2,1,0:T(8,128)(2,1)S(1)} %shard_map.238), channel_id=1, source_target_pairs={{0,3},{1,0},{2,1},{3,2},{4,7},{5,4},{6,5},{7,6},{8,11},{9,8},{10,9... | collective-permute-start | bytes 73736 | tf_op jit(solution)/shard_map/ppermute | solution.py:362
  133.8 2.8 %collective-permute-start.4 = (bf16[1,96,128]{2,1,0:T(8,128)(2,1)S(1)}, bf16[1,96,128]{2,1,0:T(8,128)(2,1)S(1)}, u32[]{:S(2)}, u32[]{:S(2)}) collective-permute-start(bf16[1,96,128]{2,1,0:T(8,128)(2,1)S(1)} %shard_map.238), channel_id=1, source_target_pairs={{0,2},{1,3},{2,0},{3,1},{4,6},{5,7},{6,4},{7,5},{8,10},{9,11},{10,... | collective-permute-start | bytes 73736 | tf_op jit(solution)/shard_map/ppermute | solution.py:362
  136.6 2.8 %collective-permute-start.3 = (bf16[1,96,128]{2,1,0:T(8,128)(2,1)S(1)}, bf16[1,96,128]{2,1,0:T(8,128)(2,1)S(1)}, u32[]{:S(2)}, u32[]{:S(2)}) collective-permute-start(bf16[1,96,128]{2,1,0:T(8,128)(2,1)S(1)} %shard_map.238), channel_id=1, source_target_pairs={{0,1},{1,2},{2,3},{3,0},{4,5},{5,6},{6,7},{7,4},{8,9},{9,10},{10,1... | collective-permute-start | bytes 73736 | tf_op jit(solution)/shard_map/ppermute | solution.py:362
  139.4 1.7 %collective-permute-done.4 = bf16[1,96,128]{2,1,0:T(8,128)(2,1)S(1)} collective-permute-done((bf16[1,96,128]{2,1,0:T(8,128)(2,1)S(1)}, bf16[1,96,128]{2,1,0:T(8,128)(2,1)S(1)}, u32[]{:S(2)}, u32[]{:S(2)}) %collective-permute-start.4) | collective-permute-done | bytes 24608 | tf_op jit(solution)/shard_map/ppermute | solution.py:362
  141.0 2.5 %collective-permute-done.3 = bf16[1,96,128]{2,1,0:T(8,128)(2,1)S(1)} collective-permute-done((bf16[1,96,128]{2,1,0:T(8,128)(2,1)S(1)}, bf16[1,96,128]{2,1,0:T(8,128)(2,1)S(1)}, u32[]{:S(2)}, u32[]{:S(2)}) %collective-permute-start.3) | collective-permute-done | bytes 24608 | tf_op jit(solution)/shard_map/ppermute | solution.py:362
  143.6 2.6 %collective-permute-start.6 = (bf16[4,96,128]{2,1,0:T(8,128)(2,1)S(1)}, bf16[4,96,128]{2,1,0:T(8,128)(2,1)S(1)}, u32[]{:S(2)}, u32[]{:S(2)}) collective-permute-start(bf16[4,96,128]{2,1,0:T(8,128)(2,1)S(1)} %pad_maximum_fusion.rest_0_), channel_id=1, source_target_pairs={{0,4},{4,8},{8,12},{12,0},{1,5},{5,9},{9,13},{13,1},{2,6},{6,10},{... | collective-permute-start | bytes 294920 | tf_op jit(solution)/shard_map/ppermute | solution.py:366
  146.2 4.5 %collective-permute-start.7 = (bf16[4,96,128]{2,1,0:T(8,128)(2,1)S(1)}, bf16[4,96,128]{2,1,0:T(8,128)(2,1)S(1)}, u32[]{:S(2)}, u32[]{:S(2)}) collective-permute-start(bf16[4,96,128]{2,1,0:T(8,128)(2,1)S(1)} %pad_maximum_fusion.rest_0_), channel_id=1, source_target_pairs={{0,8},{4,12},{8,0},{12,4},{1,9},{5,13},{9,1},{13,5},{2,10},{6,14},... | collective-permute-start | bytes 294920 | tf_op jit(solution)/shard_map/ppermute | solution.py:366
  150.7 2.3 %collective-permute-start.8 = (bf16[4,96,128]{2,1,0:T(8,128)(2,1)S(1)}, bf16[4,96,128]{2,1,0:T(8,128)(2,1)S(1)}, u32[]{:S(2)}, u32[]{:S(2)}) collective-permute-start(bf16[4,96,128]{2,1,0:T(8,128)(2,1)S(1)} %pad_maximum_fusion.rest_0_), channel_id=1, source_target_pairs={{0,12},{4,0},{8,4},{12,8},{1,13},{5,1},{9,5},{13,9},{2,14},{6,2},{... | collective-permute-start | bytes 294920 | tf_op jit(solution)/shard_map/ppermute | solution.py:366
  153.0 1.2 collective-permute-done.7.rest_2_
  154.2 3.0 %collective-permute-done.8.rest_3_ = bf16[4,96,128]{2,1,0:T(8,128)(2,1)S(1)} collective-permute-done((bf16[4,96,128]{2,1,0:T(8,128)(2,1)S(1)}, bf16[4,96,128]{2,1,0:T(8,128)(2,1)S(1)}, u32[]{:S(2)}, u32[]{:S(2)}) %collective-permute-start.8) | collective-permute-done | bytes 98336 | tf_op jit(solution)/shard_map/ppermute | solution.py:366
  157.2 1.5 shard_map.239
  (51 shorter events, 6.8 us)
Async XLA Ops:
  7.3 1.0 copy-start.3
  8.3 0.9 copy-start.7
  9.2 0.9 copy-start.8
  10.1 0.7 copy-start.11
  11.5 29.7 %copy-start.14 = (bf16[384,384]{1,0:T(8,128)(2,1)S(1)}, bf16[384,384]{1,0:T(8,128)(2,1)}, u32[]{:S(2)}) copy-start(bf16[384,384]{1,0:T(8,128)(2,1)} %constant.63.clone.order) | copy-start | bytes 884740
  46.6 32.2 %all-to-all-start.2 = ((bf16[16,384,128]{2,1,0:T(8,128)(2,1)}), bf16[16,384,128]{2,1,0:T(8,128)(2,1)S(1)}, u32[]{:S(2)}, u32[]{:S(2)}) async-start(bf16[16,384,128]{2,1,0:T(8,128)(2,1)} %shard_map.232), calls=%async_computation.2 | async-start | bytes 3145728 | tf_op jit(solution)/shard_map/all_to_all | solution.py:220
  53.7 71.4 %all-gather.2.cloned.1.call-start = ((), (), s32[]{:S(2)}) async-start(), calls=%async_computation.6 | async-start | bytes 1351680 | tf_op jit(solution)/shard_map/all_gather | solution.py:280
  53.7 25.1 %copy-start = (bf16[1,2048,256]{2,1,0:T(8,128)(2,1)S(1)}, bf16[1,2048,256]{2,1,0:T(8,128)(2,1)}, u32[]{:S(2)}) copy-start(bf16[1,2048,256]{2,1,0:T(8,128)(2,1)} %param.37) | copy-start | bytes 3145732
  78.9 1.2 copy-start.1
  82.0 3.7 %copy-start.17 = (bf16[1,4096,128]{2,1,0:T(8,128)(2,1)S(1)}, bf16[1,4096,128]{2,1,0:T(8,128)(2,1)}, u32[]{:S(2)}) copy-start(bf16[1,4096,128]{2,1,0:T(8,128)(2,1)} %param.39) | copy-start | bytes 3145732
  82.0 22.3 %all-to-all-start.3 = ((bf16[4,384,256]{2,1,0:T(8,128)(2,1)}), bf16[4,384,256]{2,1,0:T(8,128)(2,1)S(1)}, u32[]{:S(2)}, u32[]{:S(2)}) async-start(bf16[4,384,256]{2,1,0:T(8,128)(2,1)} %shard_map.233), calls=%async_computation.3 | async-start | bytes 1572864 | tf_op jit(solution)/shard_map/all_to_all | solution.py:220
  85.8 16.0 %collective-permute-start = (bf16[1024,128]{1,0:T(8,128)(2,1)S(1)}, bf16[1024,128]{1,0:T(8,128)(2,1)S(1)}, u32[]{:S(2)}, u32[]{:S(2)}) collective-permute-start(bf16[1024,128]{1,0:T(8,128)(2,1)S(1)} %get-tuple-element.9), channel_id=1, source_target_pairs={{0,4},{4,8},{8,12},{12,0},{1,5},{5,9},{9,13},{13,1},{2,6},{6,10},{... | collective-permute-start | bytes 786440 | tf_op jit(solution)/shard_map/ppermute | solution.py:287
  88.0 13.8 %collective-permute-start.1 = (bf16[1024,128]{1,0:T(8,128)(2,1)S(1)}, bf16[1024,128]{1,0:T(8,128)(2,1)S(1)}, u32[]{:S(2)}, u32[]{:S(2)}) collective-permute-start(bf16[1024,128]{1,0:T(8,128)(2,1)S(1)} %get-tuple-element.11), channel_id=1, source_target_pairs={{0,8},{4,12},{8,0},{12,4},{1,9},{5,13},{9,1},{13,5},{2,10},{6,14},... | collective-permute-start | bytes 786440 | tf_op jit(solution)/shard_map/ppermute | solution.py:287
  92.5 11.8 %collective-permute-start.2 = (bf16[1024,128]{1,0:T(8,128)(2,1)S(1)}, bf16[1024,128]{1,0:T(8,128)(2,1)S(1)}, u32[]{:S(2)}, u32[]{:S(2)}) collective-permute-start(bf16[1024,128]{1,0:T(8,128)(2,1)S(1)} %get-tuple-element.8), channel_id=1, source_target_pairs={{0,12},{4,0},{8,4},{12,8},{1,13},{5,1},{9,5},{13,9},{2,14},{6,2},{... | collective-permute-start | bytes 786440 | tf_op jit(solution)/shard_map/ppermute | solution.py:287
  104.3 6.2 %copy-start.18 = (f32[1536]{0:T(1024)S(1)}, f32[1536]{0:T(1024)}, u32[]{:S(2)}) copy-start(f32[1536]{0:T(1024)} %param.26) | copy-start | bytes 18436
  106.6 12.1 %all-to-all-start.4 = ((bf16[8,192,128]{2,1,0:T(8,128)(2,1)}), bf16[8,192,128]{2,1,0:T(8,128)(2,1)S(1)}, u32[]{:S(2)}, u32[]{:S(2)}) async-start(bf16[8,192,128]{2,1,0:T(8,128)(2,1)} %bitcast.20), calls=%async_computation.4 | async-start | bytes 786432 | tf_op jit(solution)/shard_map/all_to_all | solution.py:220
  118.7 5.1 %copy-start.4 = (bf16[128,1536]{1,0:T(8,128)(2,1)S(1)}, bf16[128,1536]{1,0:T(8,128)(2,1)}, u32[]{:S(2)}) copy-start(bf16[128,1536]{1,0:T(8,128)(2,1)} %latent.2) | copy-start | bytes 1179652
  118.7 5.1 %copy-start.6 = (bf16[1536,64]{0,1:T(8,128)(2,1)S(1)}, bf16[1536,64]{0,1:T(8,128)(2,1)}, u32[]{:S(2)}) copy-start(bf16[1536,64]{0,1:T(8,128)(2,1)} %param.28) | copy-start | bytes 589828
  118.7 5.1 %copy-start.10 = (bf16[1536,32]{0,1:T(8,128)(2,1)S(1)}, bf16[1536,32]{0,1:T(8,128)(2,1)}, u32[]{:S(2)}) copy-start(bf16[1536,32]{0,1:T(8,128)(2,1)} %param.29) | copy-start | bytes 294916
  118.7 5.1 %copy-start.15 = (f32[32,16,128]{2,1,0:T(8,128)S(1)}, f32[32,16,128]{2,1,0:T(8,128)}, u32[]{:S(2)}) copy-start(f32[32,16,128]{2,1,0:T(8,128)} %constant.64.clone.cos) | copy-start | bytes 786436
  118.7 5.1 %copy-start.16 = (f32[32,16,128]{2,1,0:T(8,128)S(1)}, f32[32,16,128]{2,1,0:T(8,128)}, u32[]{:S(2)}) copy-start(f32[32,16,128]{2,1,0:T(8,128)} %constant.65.clone.sin) | copy-start | bytes 786436
  119.7 37.6 %all-to-all-start.5 = ((bf16[16,24,128]{2,1,0:T(8,128)(2,1)}), bf16[16,24,128]{2,1,0:T(8,128)(2,1)S(1)}, u32[]{:S(2)}, u32[]{:S(2)}) async-start(bf16[16,24,128]{2,1,0:T(8,128)(2,1)} %bitcast.22), calls=%async_computation.5 | async-start | bytes 196608 | tf_op jit(solution)/shard_map/all_to_all | solution.py:220
  125.1 1.3 copy-start.2
  126.4 30.8 %copy-start.5 = (bf16[1024,128]{1,0:T(8,128)(2,1)S(1)}, bf16[1024,128]{1,0:T(8,128)(2,1)}, u32[]{:S(2)}) copy-start(bf16[1024,128]{1,0:T(8,128)(2,1)} %output_weight.1) | copy-start | bytes 786436
  126.4 30.8 %copy-start.9 = (bf16[512,128]{1,0:T(8,128)(2,1)S(1)}, bf16[512,128]{1,0:T(8,128)(2,1)}, u32[]{:S(2)}) copy-start(bf16[512,128]{1,0:T(8,128)(2,1)} %shared_down.1) | copy-start | bytes 393220
  126.4 30.9 %copy-start.13 = (f32[128,2]{0,1:T(2,128)S(1)}, f32[128,2]{0,1:T(2,128)}, u32[]{:S(2)}) copy-start(f32[128,2]{0,1:T(2,128)} %param.36) | copy-start | bytes 3076
  129.1 10.3 %collective-permute-start.5 = (bf16[1,96,128]{2,1,0:T(8,128)(2,1)S(1)}, bf16[1,96,128]{2,1,0:T(8,128)(2,1)S(1)}, u32[]{:S(2)}, u32[]{:S(2)}) collective-permute-start(bf16[1,96,128]{2,1,0:T(8,128)(2,1)S(1)} %shard_map.238), channel_id=1, source_target_pairs={{0,3},{1,0},{2,1},{3,2},{4,7},{5,4},{6,5},{7,6},{8,11},{9,8},{10,9... | collective-permute-start | bytes 73736 | tf_op jit(solution)/shard_map/ppermute | solution.py:362
  133.8 7.2 %collective-permute-start.4 = (bf16[1,96,128]{2,1,0:T(8,128)(2,1)S(1)}, bf16[1,96,128]{2,1,0:T(8,128)(2,1)S(1)}, u32[]{:S(2)}, u32[]{:S(2)}) collective-permute-start(bf16[1,96,128]{2,1,0:T(8,128)(2,1)S(1)} %shard_map.238), channel_id=1, source_target_pairs={{0,2},{1,3},{2,0},{3,1},{4,6},{5,7},{6,4},{7,5},{8,10},{9,11},{10,... | collective-permute-start | bytes 73736 | tf_op jit(solution)/shard_map/ppermute | solution.py:362
  136.6 6.9 %collective-permute-start.3 = (bf16[1,96,128]{2,1,0:T(8,128)(2,1)S(1)}, bf16[1,96,128]{2,1,0:T(8,128)(2,1)S(1)}, u32[]{:S(2)}, u32[]{:S(2)}) collective-permute-start(bf16[1,96,128]{2,1,0:T(8,128)(2,1)S(1)} %shard_map.238), channel_id=1, source_target_pairs={{0,1},{1,2},{2,3},{3,0},{4,5},{5,6},{6,7},{7,4},{8,9},{9,10},{10,1... | collective-permute-start | bytes 73736 | tf_op jit(solution)/shard_map/ppermute | solution.py:362
  143.6 9.5 %collective-permute-start.6 = (bf16[4,96,128]{2,1,0:T(8,128)(2,1)S(1)}, bf16[4,96,128]{2,1,0:T(8,128)(2,1)S(1)}, u32[]{:S(2)}, u32[]{:S(2)}) collective-permute-start(bf16[4,96,128]{2,1,0:T(8,128)(2,1)S(1)} %pad_maximum_fusion.rest_0_), channel_id=1, source_target_pairs={{0,4},{4,8},{8,12},{12,0},{1,5},{5,9},{9,13},{13,1},{2,6},{6,10},{... | collective-permute-start | bytes 294920 | tf_op jit(solution)/shard_map/ppermute | solution.py:366
  146.2 8.0 %collective-permute-start.7 = (bf16[4,96,128]{2,1,0:T(8,128)(2,1)S(1)}, bf16[4,96,128]{2,1,0:T(8,128)(2,1)S(1)}, u32[]{:S(2)}, u32[]{:S(2)}) collective-permute-start(bf16[4,96,128]{2,1,0:T(8,128)(2,1)S(1)} %pad_maximum_fusion.rest_0_), channel_id=1, source_target_pairs={{0,8},{4,12},{8,0},{12,4},{1,9},{5,13},{9,1},{13,5},{2,10},{6,14},... | collective-permute-start | bytes 294920 | tf_op jit(solution)/shard_map/ppermute | solution.py:366
  150.7 6.5 %collective-permute-start.8 = (bf16[4,96,128]{2,1,0:T(8,128)(2,1)S(1)}, bf16[4,96,128]{2,1,0:T(8,128)(2,1)S(1)}, u32[]{:S(2)}, u32[]{:S(2)}) collective-permute-start(bf16[4,96,128]{2,1,0:T(8,128)(2,1)S(1)} %pad_maximum_fusion.rest_0_), channel_id=1, source_target_pairs={{0,12},{4,0},{8,4},{12,8},{1,13},{5,1},{9,5},{13,9},{2,14},{6,2},{... | collective-permute-start | bytes 294920 | tf_op jit(solution)/shard_map/ppermute | solution.py:366
  (1 other events, 0.7 us)
Sparse Core Ops, SparseCore 0:
  56.6 63.8 all-gather.1

commit v4 on v3

--- a/solution.py
+++ b/solution.py
@@ -56,8 +56,8 @@
 
 def key_value_kernel(latent, scaling, key_up, value_up, rotary, out):
     context = rms(latent[...], scaling[...])
-    out[0:PLAIN, :] = dot(key_up[...], context, 1, 1).astype(BF16)
-    out[PLAIN : PLAIN + VALUE, :] = dot(value_up[...], context, 1, 1).astype(BF16)
+    both = jnp.concatenate([key_up[...], value_up[...]], axis=0)
+    out[0 : PLAIN + VALUE, :] = dot(both, context, 1, 1).astype(BF16)
     out[PLAIN + VALUE :, :] = rotary[...]
 
 
@@ -74,32 +74,38 @@
 
 
 def attention_kernel(query, kv, shared, cos, sin, out, scores):
+    blocks, _, width = kv.shape
     q = query[...]
-    blocks, _, width = kv.shape
     half = ROTARY // 2
     scale = (PLAIN + ROTARY) ** -0.5
     tokens = q.shape[0]
 
-    top = jnp.full((tokens, width), -jnp.inf, F32)
-    for j in range(blocks):
+    def keys(j):
         raw = kv[j, PLAIN + VALUE :, :].astype(F32)
         a, b = raw[0:half, :], raw[half:, :]
         c, s = cos[j], sin[j]
         high, middle, low = split3(jnp.concatenate([a * c - b * s, a * s + b * c], axis=0))
-        keys = jnp.concatenate(
+        return jnp.concatenate(
             [kv[j, 0:PLAIN, :], high, middle, high, middle, low, high], axis=0
         )
-        part = dot(q, keys) * scale
-        scores[:, j * width : (j + 1) * width] = part
+
+    def place(j):
+        return slice(j * width, (j + 2) * width)
+
+    top = jnp.full((tokens, 2 * width), -jnp.inf, F32)
+    for j in range(0, blocks, 2):
+        part = dot(q, jnp.concatenate([keys(j), keys(j + 1)], axis=1)) * scale
+        scores[:, place(j)] = part
         top = jnp.maximum(top, part)
     largest = jnp.max(top, axis=1, keepdims=True)
-    total = jnp.zeros((tokens, width), F32)
+    total = jnp.zeros((tokens, 2 * width), F32)
     summed = jnp.zeros((VALUE, tokens), F32)
-    for j in range(blocks):
-        weights = jnp.exp(scores[:, j * width : (j + 1) * width] - largest)
+    for j in range(0, blocks, 2):
+        weights = jnp.exp(scores[:, place(j)] - largest)
         total = total + weights
-        summed = summed + dot(kv[j, PLAIN : PLAIN + VALUE, :], weights.astype(BF16), 1, 1)
-    whole = jnp.broadcast_to(jnp.sum(total, axis=1, keepdims=True), (tokens, width)).T
+        values = [kv[k, PLAIN : PLAIN + VALUE, :] for k in (j, j + 1)]
+        summed = summed + dot(jnp.concatenate(values, axis=1), weights.astype(BF16), 1, 1)
+    whole = jnp.broadcast_to(jnp.sum(total, axis=1, keepdims=True), (tokens, tokens)).T
     heads = (summed / whole[0:VALUE, :]).astype(BF16)
     out[0] = jnp.concatenate([heads, shared[...]], axis=0)
 
@@ -161,11 +167,13 @@
     downs, out = rest[:-1], rest[-1]
     parts, tall, length = out.shape[0], out.shape[1], out.shape[2]
     x = jnp.concatenate([hidden[t] for t in range(hidden.shape[0])], axis=1)
-    for k, down in enumerate(downs):
+    result = dot(x, jnp.concatenate([down[...] for down in downs], axis=1)).astype(BF16)
+    width = out.shape[3]
+    for k in range(tall):
         to = (place[4] + (tall - k)) % tall
-        result = dot(x, down[...]).astype(BF16)
         for c in range(parts):
-            out[c, to] = result[c * length : (c + 1) * length, :]
+            rows = slice(c * length, (c + 1) * length)
+            out[c, to] = result[rows, k * width : (k + 1) * width]
 
 
 def gathered_sum_kernel(order, partial, out):

time: 167 us -> 165 us (0.988)
  transfers between devices with their start and end apart: 14 -> 14, of which waited for: 8 -> 8; matrix products, arithmetic and copies ran while one was open for 0% -> 0% of each run, Pallas kernels for 7% -> 6%
where the time goes in v4:
time: 165 us; the launch traced here: 164 us
  waiting for transfers between devices  49 us (30%)
  starting transfers between devices  47.7 us (29%)
  blocking collectives  31.8 us (19%)
  Pallas kernels  14.4 us (9%)
  between operations  14.4 us (9%)
  local copies, waits for them, and re-layouts  6.98 us (4%)
    all_to_all x2, blocking collectives, exchange(): return lax.all_to_all(array, axes, 0, 0, tiled=True)  31.8 us
    all_to_all x4, waiting for transfers between devices, exchange(): return lax.all_to_all(array, axes, 0, 0, tiled=True)  31.3 us
    all_to_all x4, starting transfers between devices, exchange(): return lax.all_to_all(array, axes, 0, 0, tiled=True)  18.7 us
    pallas_call x10, Pallas kernels, call(): pl.pallas_call(body, out_shape=outs, in_specs=[SMEM] * smem + [VMEM] * (l...  14.4 us
    ppermute x3, starting transfers between devices, per_device(): lax.ppermute(both, 'x', [(x, (x + k) % across) for x in range(across)])  10.3 us
    ppermute x3, starting transfers between devices, per_device(): lax.ppermute(both, 'y', [(y, (y + k) % tall) for y in range(tall)])  9.42 us
    ppermute x3, waiting for transfers between devices, per_device(): part = lax.ppermute(part, 'y', [(y, (y + k) % tall) for y in range(tall)])  9.3 us
    ppermute x3, starting transfers between devices, per_device(): part = lax.ppermute(part, 'y', [(y, (y + k) % tall) for y in range(tall)])  9.2 us
  transfers between devices with their start and end apart: 14, of which 8 were waited for; matrix products, arithmetic and copies ran while one was open for 0% of the time, Pallas kernels for 6%

profile of v4, /device:TPU:32, one launch (start us, length us, event | category | flops | bytes accessed | tf_op | source)
XLA Modules:
  0.0 164.2 jit_solution(16559990628479324386)
XLA Ops:
  11.5 1.7 %shard_map.230 = (bf16[384,128]{1,0:T(8,128)(2,1)S(1)}, s32[2,128]{1,0:T(2,128)S(1)}, bf16[32,128]{1,0:T(8,128)(2,1)S(1)}, bf16[128,2048]{1,0:T(8,128)(2,1)}) custom-call(s32[6]{0:T(128)S(1)} %stack.27.place, bf16[128,2048]{1,0:T(8,128)(2,1)S(1)} %copy-done.3, f32[1,2048]{1,0:T(1,128)S(1)} %bitcast.49, s32[2,128]{1,0:T(2,128)S(1)} %bitcast.50, ...), custom_call_target="tpu_custom_call" | custom-call | flops 1000000000 | bytes 1000000 | tf_op jit(solution)/shard_map/pallas_call | solution.py:28
  13.2 28.0 %all_to_all.30 = bf16[16,24,128]{2,1,0:T(8,128)(2,1)S(1)} all-to-all(bf16[16,24,128]{2,1,0:T(8,128)(2,1)S(1)} %bitcast.40), channel_id=1, replica_groups=mesh['z'=16,'core'=2,'y'=4,'x'=4] {'z'}, dimensions={0} | all-to-all | bytes 196608 | tf_op jit(solution)/shard_map/all_to_all | solution.py:228
  41.5 3.8 %all_to_all.31 = bf16[2,192,128]{2,1,0:T(8,128)(2,1)S(1)} all-to-all(bf16[2,192,128]{2,1,0:T(8,128)(2,1)S(1)} %bitcast.42), channel_id=1, replica_groups=mesh['z'=16,'core'=2,'y'=4,'x'=4] {'core'}, dimensions={0} | all-to-all | bytes 196608 | tf_op jit(solution)/shard_map/all_to_all | solution.py:228
  45.3 1.4 shard_map.232
  46.6 7.0 %all-to-all-start.2 = ((bf16[16,384,128]{2,1,0:T(8,128)(2,1)}), bf16[16,384,128]{2,1,0:T(8,128)(2,1)S(1)}, u32[]{:S(2)}, u32[]{:S(2)}) async-start(bf16[16,384,128]{2,1,0:T(8,128)(2,1)} %shard_map.232), calls=%async_computation.2 | async-start | bytes 3145728 | tf_op jit(solution)/shard_map/all_to_all | solution.py:228
  53.7 1.9 %shard_map.237 = bf16[160,128]{1,0:T(8,128)(2,1)} custom-call(bf16[128,512]{1,0:T(8,128)(2,1)} %latent.3, f32[1,512]{1,0:T(1,128)} %bitcast.55, bf16[64,512]{1,0:T(8,128)(2,1)} %bitcast.52, bf16[64,512]{1,0:T(8,128)(2,1)} %bitcast.53, bf16[32,128]{1,0:T(8,128)(2,1)} %bitcast.54), custom_call_target="tpu_custom_call" | custom-call | flops 1000000000 | bytes 1000000 | tf_op jit(solution)/shard_map/pallas_call | solution.py:28
  55.7 23.1 %all-to-all-done.2.rows = bf16[16,384,128]{2,1,0:T(8,128)(2,1)S(1)} async-done(((bf16[16,384,128]{2,1,0:T(8,128)(2,1)}), bf16[16,384,128]{2,1,0:T(8,128)(2,1)S(1)}, u32[]{:S(2)}, u32[]{:S(2)}) %all-to-all-start.2) | async-done | bytes 1572896 | tf_op jit(solution)/shard_map/all_to_all | solution.py:228
  78.9 1.2 copy-done.1
  80.1 1.9 %shard_map.233 = bf16[4,384,256]{2,1,0:T(8,128)(2,1)} custom-call(bf16[16,384,128]{2,1,0:T(8,128)(2,1)S(1)} %all-to-all-done.2.rows, bf16[2048,256]{1,0:T(8,128)(2,1)S(1)} %bitcast.36, bf16[2048,256]{1,0:T(8,128)(2,1)S(1)} %bitcast.37), custom_call_target="tpu_custom_call" | custom-call | flops 1000000000 | bytes 1000000 | tf_op jit(solution)/shard_map/pallas_call | solution.py:28
  82.0 3.6 %all-to-all-start.3 = ((bf16[4,384,256]{2,1,0:T(8,128)(2,1)}), bf16[4,384,256]{2,1,0:T(8,128)(2,1)S(1)}, u32[]{:S(2)}, u32[]{:S(2)}) async-start(bf16[4,384,256]{2,1,0:T(8,128)(2,1)} %shard_map.233), calls=%async_computation.3 | async-start | bytes 1572864 | tf_op jit(solution)/shard_map/all_to_all | solution.py:228
  85.8 2.2 %collective-permute-start = (bf16[1024,128]{1,0:T(8,128)(2,1)S(1)}, bf16[1024,128]{1,0:T(8,128)(2,1)S(1)}, u32[]{:S(2)}, u32[]{:S(2)}) collective-permute-start(bf16[1024,128]{1,0:T(8,128)(2,1)S(1)} %get-tuple-element.9), channel_id=1, source_target_pairs={{0,4},{4,8},{8,12},{12,0},{1,5},{5,9},{9,13},{13,1},{2,6},{6,10},{... | collective-permute-start | bytes 786440 | tf_op jit(solution)/shard_map/ppermute | solution.py:295
  88.0 4.5 %collective-permute-start.1 = (bf16[1024,128]{1,0:T(8,128)(2,1)S(1)}, bf16[1024,128]{1,0:T(8,128)(2,1)S(1)}, u32[]{:S(2)}, u32[]{:S(2)}) collective-permute-start(bf16[1024,128]{1,0:T(8,128)(2,1)S(1)} %get-tuple-element.11), channel_id=1, source_target_pairs={{0,8},{4,12},{8,0},{12,4},{1,9},{5,13},{9,1},{13,5},{2,10},{6,14},... | collective-permute-start | bytes 786440 | tf_op jit(solution)/shard_map/ppermute | solution.py:295
  92.5 2.5 %collective-permute-start.2 = (bf16[1024,128]{1,0:T(8,128)(2,1)S(1)}, bf16[1024,128]{1,0:T(8,128)(2,1)S(1)}, u32[]{:S(2)}, u32[]{:S(2)}) collective-permute-start(bf16[1024,128]{1,0:T(8,128)(2,1)S(1)} %get-tuple-element.8), channel_id=1, source_target_pairs={{0,12},{4,0},{8,4},{12,8},{1,13},{5,1},{9,5},{13,9},{2,14},{6,2},{... | collective-permute-start | bytes 786440 | tf_op jit(solution)/shard_map/ppermute | solution.py:295
  95.0 6.8 %collective-permute-done.rest_1_ = bf16[1024,128]{1,0:T(8,128)(2,1)S(1)} collective-permute-done((bf16[1024,128]{1,0:T(8,128)(2,1)S(1)}, bf16[1024,128]{1,0:T(8,128)(2,1)S(1)}, u32[]{:S(2)}, u32[]{:S(2)}) %collective-permute-start) | collective-permute-done | bytes 262176 | tf_op jit(solution)/shard_map/ppermute | solution.py:295
  101.8 2.5 %collective-permute-done.2.rest_3_ = bf16[1024,128]{1,0:T(8,128)(2,1)S(1)} collective-permute-done((bf16[1024,128]{1,0:T(8,128)(2,1)S(1)}, bf16[1024,128]{1,0:T(8,128)(2,1)S(1)}, u32[]{:S(2)}, u32[]{:S(2)}) %collective-permute-start.2) | collective-permute-done | bytes 262176 | tf_op jit(solution)/shard_map/ppermute | solution.py:295
  104.3 1.9 %shard_map.234 = bf16[2,4,192,128]{3,2,1,0:T(8,128)(2,1)} custom-call(s32[6]{0:T(128)S(1)} %stack.27.place, bf16[4,384,256]{2,1,0:T(8,128)(2,1)S(1)} %all-to-all-done.3.hidden, bf16[1024,128]{1,0:T(8,128)(2,1)S(1)} %get-tuple-element.10.rest_0_, bf16[1024,128]{1,0:T(8,128)(2,1)S(1)} %collective-permute-done.rest_1_, ...), custom_call_target="tpu_custom_call" | custom-call | flops 1000000000 | bytes 1000000 | tf_op jit(solution)/shard_map/pallas_call | solution.py:28
  106.2 3.9 %all-to-all-start.4 = ((bf16[8,192,128]{2,1,0:T(8,128)(2,1)}), bf16[8,192,128]{2,1,0:T(8,128)(2,1)S(1)}, u32[]{:S(2)}, u32[]{:S(2)}) async-start(bf16[8,192,128]{2,1,0:T(8,128)(2,1)} %bitcast.20), calls=%async_computation.4 | async-start | bytes 786432 | tf_op jit(solution)/shard_map/all_to_all | solution.py:228
  110.1 8.2 %all-to-all-done.4 = bf16[8,192,128]{2,1,0:T(8,128)(2,1)S(1)} async-done(((bf16[8,192,128]{2,1,0:T(8,128)(2,1)}), bf16[8,192,128]{2,1,0:T(8,128)(2,1)S(1)}, u32[]{:S(2)}, u32[]{:S(2)}) %all-to-all-start.4) | async-done | bytes 393248 | tf_op jit(solution)/shard_map/all_to_all | solution.py:228
  119.3 4.2 %all-to-all-start.5 = ((bf16[16,24,128]{2,1,0:T(8,128)(2,1)}), bf16[16,24,128]{2,1,0:T(8,128)(2,1)S(1)}, u32[]{:S(2)}, u32[]{:S(2)}) async-start(bf16[16,24,128]{2,1,0:T(8,128)(2,1)} %bitcast.22), calls=%async_computation.5 | async-start | bytes 196608 | tf_op jit(solution)/shard_map/all_to_all | solution.py:228
  124.7 1.3 copy-done.2
  126.0 1.7 %shard_map.238 = bf16[1,96,128]{2,1,0:T(8,128)(2,1)S(1)} custom-call(bf16[128,256]{1,0:T(8,128)(2,1)S(1)} %shard_map.236.query, bf16[32,160,128]{2,1,0:T(8,128)(2,1)S(1)} %bitcast.44, bf16[32,128]{1,0:T(8,128)(2,1)S(1)} %get-tuple-element.7.shared, f32[32,16,128]{2,1,0:T(8,128)S(1)} %copy-done.15, f32[32,16,128]{2,1,0:T(8,128)S(1)} %copy-done.16), custom_call_target="tpu_custom_call" | custom-call | flops 1000000000 | bytes 1000000 | tf_op jit(solution)/shard_map/pallas_call | solution.py:28
  127.7 4.8 %collective-permute-start.5 = (bf16[1,96,128]{2,1,0:T(8,128)(2,1)S(1)}, bf16[1,96,128]{2,1,0:T(8,128)(2,1)S(1)}, u32[]{:S(2)}, u32[]{:S(2)}) collective-permute-start(bf16[1,96,128]{2,1,0:T(8,128)(2,1)S(1)} %shard_map.238), channel_id=1, source_target_pairs={{0,3},{1,0},{2,1},{3,2},{4,7},{5,4},{6,5},{7,6},{8,11},{9,8},{10,9... | collective-permute-start | bytes 73736 | tf_op jit(solution)/shard_map/ppermute | solution.py:370
  132.4 2.8 %collective-permute-start.4 = (bf16[1,96,128]{2,1,0:T(8,128)(2,1)S(1)}, bf16[1,96,128]{2,1,0:T(8,128)(2,1)S(1)}, u32[]{:S(2)}, u32[]{:S(2)}) collective-permute-start(bf16[1,96,128]{2,1,0:T(8,128)(2,1)S(1)} %shard_map.238), channel_id=1, source_target_pairs={{0,2},{1,3},{2,0},{3,1},{4,6},{5,7},{6,4},{7,5},{8,10},{9,11},{10,... | collective-permute-start | bytes 73736 | tf_op jit(solution)/shard_map/ppermute | solution.py:370
  135.2 2.8 %collective-permute-start.3 = (bf16[1,96,128]{2,1,0:T(8,128)(2,1)S(1)}, bf16[1,96,128]{2,1,0:T(8,128)(2,1)S(1)}, u32[]{:S(2)}, u32[]{:S(2)}) collective-permute-start(bf16[1,96,128]{2,1,0:T(8,128)(2,1)S(1)} %shard_map.238), channel_id=1, source_target_pairs={{0,1},{1,2},{2,3},{3,0},{4,5},{5,6},{6,7},{7,4},{8,9},{9,10},{10,1... | collective-permute-start | bytes 73736 | tf_op jit(solution)/shard_map/ppermute | solution.py:370
  138.0 1.7 %collective-permute-done.4 = bf16[1,96,128]{2,1,0:T(8,128)(2,1)S(1)} collective-permute-done((bf16[1,96,128]{2,1,0:T(8,128)(2,1)S(1)}, bf16[1,96,128]{2,1,0:T(8,128)(2,1)S(1)}, u32[]{:S(2)}, u32[]{:S(2)}) %collective-permute-start.4) | collective-permute-done | bytes 24608 | tf_op jit(solution)/shard_map/ppermute | solution.py:370
  139.7 2.5 %collective-permute-done.3 = bf16[1,96,128]{2,1,0:T(8,128)(2,1)S(1)} collective-permute-done((bf16[1,96,128]{2,1,0:T(8,128)(2,1)S(1)}, bf16[1,96,128]{2,1,0:T(8,128)(2,1)S(1)}, u32[]{:S(2)}, u32[]{:S(2)}) %collective-permute-start.3) | collective-permute-done | bytes 24608 | tf_op jit(solution)/shard_map/ppermute | solution.py:370
  142.2 2.6 %collective-permute-start.6 = (bf16[4,96,128]{2,1,0:T(8,128)(2,1)S(1)}, bf16[4,96,128]{2,1,0:T(8,128)(2,1)S(1)}, u32[]{:S(2)}, u32[]{:S(2)}) collective-permute-start(bf16[4,96,128]{2,1,0:T(8,128)(2,1)S(1)} %pad_maximum_fusion.rest_0_), channel_id=1, source_target_pairs={{0,4},{4,8},{8,12},{12,0},{1,5},{5,9},{9,13},{13,1},{2,6},{6,10},{... | collective-permute-start | bytes 294920 | tf_op jit(solution)/shard_map/ppermute | solution.py:374
  144.8 4.5 %collective-permute-start.7 = (bf16[4,96,128]{2,1,0:T(8,128)(2,1)S(1)}, bf16[4,96,128]{2,1,0:T(8,128)(2,1)S(1)}, u32[]{:S(2)}, u32[]{:S(2)}) collective-permute-start(bf16[4,96,128]{2,1,0:T(8,128)(2,1)S(1)} %pad_maximum_fusion.rest_0_), channel_id=1, source_target_pairs={{0,8},{4,12},{8,0},{12,4},{1,9},{5,13},{9,1},{13,5},{2,10},{6,14},... | collective-permute-start | bytes 294920 | tf_op jit(solution)/shard_map/ppermute | solution.py:374
  149.3 2.3 %collective-permute-start.8 = (bf16[4,96,128]{2,1,0:T(8,128)(2,1)S(1)}, bf16[4,96,128]{2,1,0:T(8,128)(2,1)S(1)}, u32[]{:S(2)}, u32[]{:S(2)}) collective-permute-start(bf16[4,96,128]{2,1,0:T(8,128)(2,1)S(1)} %pad_maximum_fusion.rest_0_), channel_id=1, source_target_pairs={{0,12},{4,0},{8,4},{12,8},{1,13},{5,1},{9,5},{13,9},{2,14},{6,2},{... | collective-permute-start | bytes 294920 | tf_op jit(solution)/shard_map/ppermute | solution.py:374
  151.6 1.2 collective-permute-done.7.rest_2_
  152.8 3.0 %collective-permute-done.8.rest_3_ = bf16[4,96,128]{2,1,0:T(8,128)(2,1)S(1)} collective-permute-done((bf16[4,96,128]{2,1,0:T(8,128)(2,1)S(1)}, bf16[4,96,128]{2,1,0:T(8,128)(2,1)S(1)}, u32[]{:S(2)}, u32[]{:S(2)}) %collective-permute-start.8) | collective-permute-done | bytes 98336 | tf_op jit(solution)/shard_map/ppermute | solution.py:374
  155.8 1.5 shard_map.239
  (51 shorter events, 6.9 us)
Async XLA Ops:
  7.3 1.0 copy-start.3
  8.3 0.9 copy-start.7
  9.2 0.9 copy-start.8
  10.1 0.7 copy-start.11
  11.5 29.7 %copy-start.14 = (bf16[384,384]{1,0:T(8,128)(2,1)S(1)}, bf16[384,384]{1,0:T(8,128)(2,1)}, u32[]{:S(2)}) copy-start(bf16[384,384]{1,0:T(8,128)(2,1)} %constant.63.clone.order) | copy-start | bytes 884740
  46.6 32.2 %all-to-all-start.2 = ((bf16[16,384,128]{2,1,0:T(8,128)(2,1)}), bf16[16,384,128]{2,1,0:T(8,128)(2,1)S(1)}, u32[]{:S(2)}, u32[]{:S(2)}) async-start(bf16[16,384,128]{2,1,0:T(8,128)(2,1)} %shard_map.232), calls=%async_computation.2 | async-start | bytes 3145728 | tf_op jit(solution)/shard_map/all_to_all | solution.py:228
  53.7 71.0 %all-gather.2.cloned.1.call-start = ((), (), s32[]{:S(2)}) async-start(), calls=%async_computation.6 | async-start | bytes 1351680 | tf_op jit(solution)/shard_map/all_gather | solution.py:288
  53.7 25.1 %copy-start = (bf16[1,2048,256]{2,1,0:T(8,128)(2,1)S(1)}, bf16[1,2048,256]{2,1,0:T(8,128)(2,1)}, u32[]{:S(2)}) copy-start(bf16[1,2048,256]{2,1,0:T(8,128)(2,1)} %param.37) | copy-start | bytes 3145732
  78.9 1.2 copy-start.1
  82.0 3.7 %copy-start.17 = (bf16[1,4096,128]{2,1,0:T(8,128)(2,1)S(1)}, bf16[1,4096,128]{2,1,0:T(8,128)(2,1)}, u32[]{:S(2)}) copy-start(bf16[1,4096,128]{2,1,0:T(8,128)(2,1)} %param.39) | copy-start | bytes 3145732
  82.0 22.3 %all-to-all-start.3 = ((bf16[4,384,256]{2,1,0:T(8,128)(2,1)}), bf16[4,384,256]{2,1,0:T(8,128)(2,1)S(1)}, u32[]{:S(2)}, u32[]{:S(2)}) async-start(bf16[4,384,256]{2,1,0:T(8,128)(2,1)} %shard_map.233), calls=%async_computation.3 | async-start | bytes 1572864 | tf_op jit(solution)/shard_map/all_to_all | solution.py:228
  85.8 16.0 %collective-permute-start = (bf16[1024,128]{1,0:T(8,128)(2,1)S(1)}, bf16[1024,128]{1,0:T(8,128)(2,1)S(1)}, u32[]{:S(2)}, u32[]{:S(2)}) collective-permute-start(bf16[1024,128]{1,0:T(8,128)(2,1)S(1)} %get-tuple-element.9), channel_id=1, source_target_pairs={{0,4},{4,8},{8,12},{12,0},{1,5},{5,9},{9,13},{13,1},{2,6},{6,10},{... | collective-permute-start | bytes 786440 | tf_op jit(solution)/shard_map/ppermute | solution.py:295
  88.0 13.8 %collective-permute-start.1 = (bf16[1024,128]{1,0:T(8,128)(2,1)S(1)}, bf16[1024,128]{1,0:T(8,128)(2,1)S(1)}, u32[]{:S(2)}, u32[]{:S(2)}) collective-permute-start(bf16[1024,128]{1,0:T(8,128)(2,1)S(1)} %get-tuple-element.11), channel_id=1, source_target_pairs={{0,8},{4,12},{8,0},{12,4},{1,9},{5,13},{9,1},{13,5},{2,10},{6,14},... | collective-permute-start | bytes 786440 | tf_op jit(solution)/shard_map/ppermute | solution.py:295
  92.5 11.8 %collective-permute-start.2 = (bf16[1024,128]{1,0:T(8,128)(2,1)S(1)}, bf16[1024,128]{1,0:T(8,128)(2,1)S(1)}, u32[]{:S(2)}, u32[]{:S(2)}) collective-permute-start(bf16[1024,128]{1,0:T(8,128)(2,1)S(1)} %get-tuple-element.8), channel_id=1, source_target_pairs={{0,12},{4,0},{8,4},{12,8},{1,13},{5,1},{9,5},{13,9},{2,14},{6,2},{... | collective-permute-start | bytes 786440 | tf_op jit(solution)/shard_map/ppermute | solution.py:295
  104.3 5.8 %copy-start.18 = (f32[1536]{0:T(1024)S(1)}, f32[1536]{0:T(1024)}, u32[]{:S(2)}) copy-start(f32[1536]{0:T(1024)} %param.26) | copy-start | bytes 18436
  106.2 12.1 %all-to-all-start.4 = ((bf16[8,192,128]{2,1,0:T(8,128)(2,1)}), bf16[8,192,128]{2,1,0:T(8,128)(2,1)S(1)}, u32[]{:S(2)}, u32[]{:S(2)}) async-start(bf16[8,192,128]{2,1,0:T(8,128)(2,1)} %bitcast.20), calls=%async_computation.4 | async-start | bytes 786432 | tf_op jit(solution)/shard_map/all_to_all | solution.py:228
  118.3 5.1 %copy-start.4 = (bf16[128,1536]{1,0:T(8,128)(2,1)S(1)}, bf16[128,1536]{1,0:T(8,128)(2,1)}, u32[]{:S(2)}) copy-start(bf16[128,1536]{1,0:T(8,128)(2,1)} %latent.2) | copy-start | bytes 1179652
  118.3 5.1 %copy-start.6 = (bf16[1536,64]{0,1:T(8,128)(2,1)S(1)}, bf16[1536,64]{0,1:T(8,128)(2,1)}, u32[]{:S(2)}) copy-start(bf16[1536,64]{0,1:T(8,128)(2,1)} %param.28) | copy-start | bytes 589828
  118.3 5.1 %copy-start.10 = (bf16[1536,32]{0,1:T(8,128)(2,1)S(1)}, bf16[1536,32]{0,1:T(8,128)(2,1)}, u32[]{:S(2)}) copy-start(bf16[1536,32]{0,1:T(8,128)(2,1)} %param.29) | copy-start | bytes 294916
  118.3 5.1 %copy-start.15 = (f32[32,16,128]{2,1,0:T(8,128)S(1)}, f32[32,16,128]{2,1,0:T(8,128)}, u32[]{:S(2)}) copy-start(f32[32,16,128]{2,1,0:T(8,128)} %constant.64.clone.cos) | copy-start | bytes 786436
  118.3 5.1 %copy-start.16 = (f32[32,16,128]{2,1,0:T(8,128)S(1)}, f32[32,16,128]{2,1,0:T(8,128)}, u32[]{:S(2)}) copy-start(f32[32,16,128]{2,1,0:T(8,128)} %constant.65.clone.sin) | copy-start | bytes 786436
  119.3 36.6 %all-to-all-start.5 = ((bf16[16,24,128]{2,1,0:T(8,128)(2,1)}), bf16[16,24,128]{2,1,0:T(8,128)(2,1)S(1)}, u32[]{:S(2)}, u32[]{:S(2)}) async-start(bf16[16,24,128]{2,1,0:T(8,128)(2,1)} %bitcast.22), calls=%async_computation.5 | async-start | bytes 196608 | tf_op jit(solution)/shard_map/all_to_all | solution.py:228
  124.7 1.3 copy-start.2
  126.0 29.8 %copy-start.5 = (bf16[1024,128]{1,0:T(8,128)(2,1)S(1)}, bf16[1024,128]{1,0:T(8,128)(2,1)}, u32[]{:S(2)}) copy-start(bf16[1024,128]{1,0:T(8,128)(2,1)} %output_weight.1) | copy-start | bytes 786436
  126.0 29.8 %copy-start.9 = (bf16[512,128]{1,0:T(8,128)(2,1)S(1)}, bf16[512,128]{1,0:T(8,128)(2,1)}, u32[]{:S(2)}) copy-start(bf16[512,128]{1,0:T(8,128)(2,1)} %shared_down.1) | copy-start | bytes 393220
  126.0 29.9 %copy-start.13 = (f32[128,2]{0,1:T(2,128)S(1)}, f32[128,2]{0,1:T(2,128)}, u32[]{:S(2)}) copy-start(f32[128,2]{0,1:T(2,128)} %param.36) | copy-start | bytes 3076
  127.7 10.3 %collective-permute-start.5 = (bf16[1,96,128]{2,1,0:T(8,128)(2,1)S(1)}, bf16[1,96,128]{2,1,0:T(8,128)(2,1)S(1)}, u32[]{:S(2)}, u32[]{:S(2)}) collective-permute-start(bf16[1,96,128]{2,1,0:T(8,128)(2,1)S(1)} %shard_map.238), channel_id=1, source_target_pairs={{0,3},{1,0},{2,1},{3,2},{4,7},{5,4},{6,5},{7,6},{8,11},{9,8},{10,9... | collective-permute-start | bytes 73736 | tf_op jit(solution)/shard_map/ppermute | solution.py:370
  132.4 7.2 %collective-permute-start.4 = (bf16[1,96,128]{2,1,0:T(8,128)(2,1)S(1)}, bf16[1,96,128]{2,1,0:T(8,128)(2,1)S(1)}, u32[]{:S(2)}, u32[]{:S(2)}) collective-permute-start(bf16[1,96,128]{2,1,0:T(8,128)(2,1)S(1)} %shard_map.238), channel_id=1, source_target_pairs={{0,2},{1,3},{2,0},{3,1},{4,6},{5,7},{6,4},{7,5},{8,10},{9,11},{10,... | collective-permute-start | bytes 73736 | tf_op jit(solution)/shard_map/ppermute | solution.py:370
  135.2 6.9 %collective-permute-start.3 = (bf16[1,96,128]{2,1,0:T(8,128)(2,1)S(1)}, bf16[1,96,128]{2,1,0:T(8,128)(2,1)S(1)}, u32[]{:S(2)}, u32[]{:S(2)}) collective-permute-start(bf16[1,96,128]{2,1,0:T(8,128)(2,1)S(1)} %shard_map.238), channel_id=1, source_target_pairs={{0,1},{1,2},{2,3},{3,0},{4,5},{5,6},{6,7},{7,4},{8,9},{9,10},{10,1... | collective-permute-start | bytes 73736 | tf_op jit(solution)/shard_map/ppermute | solution.py:370
  142.2 9.4 %collective-permute-start.6 = (bf16[4,96,128]{2,1,0:T(8,128)(2,1)S(1)}, bf16[4,96,128]{2,1,0:T(8,128)(2,1)S(1)}, u32[]{:S(2)}, u32[]{:S(2)}) collective-permute-start(bf16[4,96,128]{2,1,0:T(8,128)(2,1)S(1)} %pad_maximum_fusion.rest_0_), channel_id=1, source_target_pairs={{0,4},{4,8},{8,12},{12,0},{1,5},{5,9},{9,13},{13,1},{2,6},{6,10},{... | collective-permute-start | bytes 294920 | tf_op jit(solution)/shard_map/ppermute | solution.py:374
  144.8 8.0 %collective-permute-start.7 = (bf16[4,96,128]{2,1,0:T(8,128)(2,1)S(1)}, bf16[4,96,128]{2,1,0:T(8,128)(2,1)S(1)}, u32[]{:S(2)}, u32[]{:S(2)}) collective-permute-start(bf16[4,96,128]{2,1,0:T(8,128)(2,1)S(1)} %pad_maximum_fusion.rest_0_), channel_id=1, source_target_pairs={{0,8},{4,12},{8,0},{12,4},{1,9},{5,13},{9,1},{13,5},{2,10},{6,14},... | collective-permute-start | bytes 294920 | tf_op jit(solution)/shard_map/ppermute | solution.py:374
  149.3 6.5 %collective-permute-start.8 = (bf16[4,96,128]{2,1,0:T(8,128)(2,1)S(1)}, bf16[4,96,128]{2,1,0:T(8,128)(2,1)S(1)}, u32[]{:S(2)}, u32[]{:S(2)}) collective-permute-start(bf16[4,96,128]{2,1,0:T(8,128)(2,1)S(1)} %pad_maximum_fusion.rest_0_), channel_id=1, source_target_pairs={{0,12},{4,0},{8,4},{12,8},{1,13},{5,1},{9,5},{13,9},{2,14},{6,2},{... | collective-permute-start | bytes 294920 | tf_op jit(solution)/shard_map/ppermute | solution.py:374
  (1 other events, 0.7 us)
Sparse Core Ops, SparseCore 0:
  56.6 63.8 all-gather.1
